TPU v7x, 32 devices: a whole 2x2x4 slice. The times are simulated.
32 devices in a mesh: fs: 16 (over z, y, core), tp: 2 (over x).
Axes of the slice: x: 2, y: 2, z: 4, core: 2. Of those that a mesh axis runs over, the one named last changes fastest.
Arguments:
- tokens: bfloat16 [16384, 2048], P(('fs', 'tp')), may hold values from -8 to 8
- pre_mix_gain: float32 [2048], replicated, may hold values from 0.1 to 1.9
- post_mix_gain: float32 [2048], replicated, may hold values from 0.1 to 1.9
- pre_ffn_gain: float32 [2048], replicated, may hold values from 0.1 to 1.9
- post_ffn_gain: float32 [2048], replicated, may hold values from 0.1 to 1.9
- w_branch: bfloat16 [2048, 1024], P('fs', 'tp'), may hold values from -0.125 to 0.125
- w_gelu: bfloat16 [2048, 1024], P('fs', 'tp'), may hold values from -0.125 to 0.125
- conv_weight: bfloat16 [4, 1024], P(None, 'tp'), may hold values from -3 to 3
- w_rec: bfloat16 [2, 8, 128, 128], P(None, 'tp'), may hold values from -0.5 to 0.5
- w_inp: bfloat16 [2, 8, 128, 128], P(None, 'tp'), may hold values from -0.5 to 0.5
- decay: float32 [2, 1024], P(None, 'tp'), may hold values from 3 to 10
- out_weight_t: bfloat16 [2048, 1024], P('fs', 'tp'), may hold values from -0.1875 to 0.1875
- w_gate: bfloat16 [2048, 3072], P('fs', 'tp'), may hold values from -0.125 to 0.125
- w_up: bfloat16 [2048, 3072], P('fs', 'tp'), may hold values from -0.125 to 0.125
- down_weight_t: bfloat16 [2048, 3072], P('fs', 'tp'), may hold values from -0.109375 to 0.109375
Outputs:
- layer_out: bfloat16 [16384, 2048], P(('fs', 'tp'))
All inputs are finite; a program needn't handle non-finite values.
Results may differ from a plain program's by a relative error of at most 0.014.
Values may be sent and summed in bfloat16 or wider, within the bound.
A program may use at most 128 MiB of HBM per device.

v0:
```python
import jax
import jax.numpy as jnp
from jax import lax
from jax.sharding import PartitionSpec as P

EPS = 1e-06


def normed(values, gain):
    factor = lax.rsqrt(jnp.mean(values * values, axis=-1, keepdims=True) + EPS)
    return values * factor * gain


def conv_short(branch, conv_weight):
    length = branch.shape[0]
    padded = jnp.pad(branch.astype(jnp.float32), ((2, 1), (0, 0)))
    weights = conv_weight.astype(jnp.float32)
    summed = weights[0] * padded[0:length]
    for offset in range(1, 4):
        summed = summed + weights[offset] * padded[offset : offset + length]
    return summed.astype(jnp.bfloat16)


def combine(earlier, later):
    return (earlier[0] * later[0], later[0] * earlier[1] + later[1])


def recurrence(conv_out, w_rec, w_inp, decay):
    length, channels = conv_out.shape
    blocks = w_rec.shape[0]
    grouped = conv_out.reshape(length, blocks, channels // blocks)
    rate_gate = jax.nn.sigmoid(
        jnp.einsum("lnc,ncd->lnd", grouped, w_rec, preferred_element_type=jnp.float32).reshape(
            length, channels
        )
    )
    inflow = jax.nn.sigmoid(
        jnp.einsum("lnc,ncd->lnd", grouped, w_inp, preferred_element_type=jnp.float32).reshape(
            length, channels
        )
    )
    log_retain = -8.0 * rate_gate * jax.nn.softplus(-decay)
    retain = jnp.exp(log_retain)
    feed = jnp.sqrt(-jnp.expm1(2.0 * log_retain)) * inflow * conv_out.astype(jnp.float32)
    unused_decay, states = lax.associative_scan(combine, (retain, feed), axis=0)
    return states


def gathered_product(normed_rows, left_weight, right_weight):
    row_piece = lax.all_gather(normed_rows, "tp", axis=0, tiled=True)
    return jnp.concatenate(
        [
            jnp.dot(row_piece, left_weight, preferred_element_type=jnp.float32),
            jnp.dot(row_piece, right_weight, preferred_element_type=jnp.float32),
        ],
        axis=1,
    )


def summed_rows(hidden, weight_t):
    return lax.psum_scatter(
        lax.dot_general(
            hidden, weight_t, (((1,), (1,)), ((), ())), preferred_element_type=jnp.float32
        ).astype(jnp.bfloat16),
        "tp",
        scatter_dimension=0,
        tiled=True,
    ).astype(jnp.float32)


def per_device(
    tokens,
    pre_mix_gain,
    post_mix_gain,
    pre_ffn_gain,
    post_ffn_gain,
    w_branch,
    w_gelu,
    conv_weight,
    w_rec,
    w_inp,
    decay,
    out_weight_t,
    w_gate,
    w_up,
    down_weight_t,
):
    branch_all, gelu_all, out_rows = (
        lax.all_gather(w_branch, "fs", axis=0, tiled=True),
        lax.all_gather(w_gelu, "fs", axis=0, tiled=True),
        lax.all_gather(out_weight_t, "fs", axis=0, tiled=True),
    )
    out_whole = lax.all_gather(out_rows, "tp", axis=1, tiled=True)
    stream = tokens.astype(jnp.float32)
    normed_in = normed(stream, pre_mix_gain).astype(jnp.bfloat16)
    both_in = gathered_product(normed_in, branch_all, gelu_all)
    channels = branch_all.shape[1]
    branch_in = both_in[:, :channels].astype(jnp.bfloat16)
    gelu_in = both_in[:, channels:].astype(jnp.bfloat16)
    conv_out = conv_short(branch_in, conv_weight)
    forward = recurrence(conv_out, w_rec[0], w_inp[0], decay[0])
    backward = jnp.flip(recurrence(jnp.flip(conv_out, 0), w_rec[1], w_inp[1], decay[1]), 0)
    mixer_hidden = (jax.nn.gelu(gelu_in.astype(jnp.float32)) * (forward + backward)).astype(
        jnp.bfloat16
    )
    own_hidden = lax.all_to_all(mixer_hidden, "tp", split_axis=0, concat_axis=1, tiled=True)
    mixer_sum = lax.dot_general(
        own_hidden, out_whole, (((1,), (1,)), ((), ())), preferred_element_type=jnp.float32
    )
    residual = (stream + normed(mixer_sum, post_mix_gain)).astype(jnp.bfloat16)
    middle = residual.astype(jnp.float32)
    normed_mid = normed(middle, pre_ffn_gain).astype(jnp.bfloat16)
    gate_all, up_all, down_all = (
        lax.all_gather(w_gate, "fs", axis=0, tiled=True),
        lax.all_gather(w_up, "fs", axis=0, tiled=True),
        lax.all_gather(down_weight_t, "fs", axis=0, tiled=True),
    )
    both_mid = gathered_product(normed_mid, gate_all, up_all)
    hidden_units = gate_all.shape[1]
    gate_proj = both_mid[:, :hidden_units]
    up_proj = both_mid[:, hidden_units:]
    ffn_hidden = (jax.nn.silu(gate_proj) * up_proj).astype(jnp.bfloat16)
    ffn_sum = summed_rows(ffn_hidden, down_all)
    return (middle + normed(ffn_sum, post_ffn_gain)).astype(jnp.bfloat16)


def solution(mesh):
    return jax.shard_map(
        per_device,
        mesh=mesh,
        in_specs=(
            P(("fs", "tp"), None),
            P(),
            P(),
            P(),
            P(),
            P("fs", "tp"),
            P("fs", "tp"),
            P(None, "tp"),
            P(None, "tp", None, None),
            P(None, "tp", None, None),
            P(None, "tp"),
            P("fs", "tp"),
            P("fs", "tp"),
            P("fs", "tp"),
            P("fs", "tp"),
        ),
        out_specs=P(("fs", "tp"), None),
        check_vma=False,
    )
```

profile of v0, /device:TPU:0, one launch (start us, length us, event | category | flops | bytes accessed | tf_op | source)
XLA Modules:
  0.0 898.2 jit_solution(10344242694818016376)
XLA Ops:
  12.7 41.0 %all-gather.16.cloned.1.call-done = bf16[2048,512]{1,0:T(8,128)(2,1)} async-done(((bf16[128,512]{1,0:T(8,128)(2,1)}), bf16[2048,512]{1,0:T(8,128)(2,1)}) %all-gather.16.cloned.1.call-update) | async-done | bytes 2097168 | tf_op jit(solution)/shard_map/all_gather | solution.py:91
  55.0 41.1 %all-gather.14.cloned.1.call-done = bf16[2048,512]{1,0:T(8,128)(2,1)} async-done(((bf16[128,512]{1,0:T(8,128)(2,1)}), bf16[2048,512]{1,0:T(8,128)(2,1)}) %all-gather.14.cloned.1.call-update) | async-done | bytes 2097168 | tf_op jit(solution)/shard_map/all_gather | solution.py:89
  96.1 57.0 %all-gather.10.cloned.1.call-done = bf16[1024,2048]{1,0:T(8,128)(2,1)} async-done(((bf16[512,2048]{1,0:T(8,128)(2,1)}), bf16[1024,2048]{1,0:T(8,128)(2,1)}) %all-gather.10.cloned.1.call-update) | async-done | bytes 4194320 | tf_op jit(solution)/shard_map/all_gather | solution.py:50
  153.1 5.2 fusion.18
  161.5 3.4 copy.41
  167.2 2.9 copy.42
  170.1 9.1 %multiply_exponential_fusion.1 = (f32[1024,512]{1,0:T(8,128)}, f32[1024,512]{1,0:T(8,128)}) fusion(f32[1024,512]{1,0:T(8,128)} %copy.41, f32[512]{0:T(512)S(1)} %bitcast.96, f32[1024,512]{1,0:T(8,128)} %copy.42, f32[512]{0:T(512)S(1)} %bitcast.93, f32[1024,512]{1,0:T(8,128)} %copy-done.1, f32[512]{0:T(512)S(1)} %bitcast.90, f32[512]{0:T(512)S(1)} %bitcast.87, ...), kind=kLoop, calls=%fused_computation.42 | loop fusion | flops 7340032 | bytes 10496000 | tf_op jit(solution)/shard_map/exp | solution.py:43
  179.2 6.3 slice.515
  185.6 6.3 slice.516
  191.8 6.3 slice.514
  198.1 6.2 slice.518
  204.3 4.3 fusion.60
  212.7 3.6 slice.520
  216.4 3.6 slice.524
  220.0 2.7 fusion.62
  222.7 2.5 slice.527
  225.2 2.5 slice.528
  227.7 2.5 slice.526
  230.2 2.5 slice.530
  264.8 5.8 add_convert_fusion
  270.5 15.5 %rev.8 = bf16[1024,512]{1,0:T(8,128)(2,1)} reverse(bf16[1024,512]{1,0:T(8,128)(2,1)} %add_convert_fusion), dimensions={0} | reverse | bytes 2097152 | tf_op jit(solution)/shard_map/jit(_flip)/rev | solution.py:102
  286.1 3.4 add_divide_fusion.1
  291.7 3.0 copy.43
  294.6 2.9 copy.44
  297.5 6.2 multiply_exponential_fusion
  303.7 6.2 slice.593
  309.9 6.3 slice.594
  316.2 6.2 slice.592
  322.4 6.3 slice.596
  328.7 4.1 fusion.61
  332.8 3.6 slice.599
  336.4 3.6 slice.600
  340.1 3.7 slice.598
  343.7 3.8 slice.602
  347.5 2.7 fusion.63
  355.2 2.5 slice.604
  357.7 2.5 slice.608
  408.4 2.5 slice.525
  410.9 2.5 slice.582
  416.8 3.7 slice.519
  421.1 6.3 slice.586
  427.4 6.4 slice.513
  469.5 2.5 slice.660
  475.4 3.7 slice.597
  479.8 6.3 slice.664
  486.1 6.4 slice.591
  507.6 4.6 pad.144
  514.6 8.8 pad.146
  525.8 4.9 pad.145
  547.4 4.6 pad.164
  554.4 8.6 pad.166
  565.5 4.7 pad.165
  570.2 4.0 add.428
  574.2 16.9 %rev.9 = f32[1024,512]{1,0:T(8,128)} reverse(f32[1024,512]{1,0:T(8,128)} %add.428), dimensions={0} | reverse | bytes 4194304 | tf_op jit(solution)/shard_map/jit(_flip)/rev | solution.py:102
  591.1 8.5 fusion.16
  601.2 17.0 %all_to_all.19 = bf16[2,512,512]{1,2,0:T(8,128)(2,1)} all-to-all(bf16[2,512,512]{1,2,0:T(8,128)(2,1)S(1)} %copy.40), channel_id=1, replica_groups=mesh['fs'=16,'tp'=2] {'tp'}, dimensions={0} | all-to-all | bytes 2097152 | tf_op jit(solution)/shard_map/all_to_all | solution.py:106
  618.1 5.0 multiply_reduce_fusion
  629.1 55.4 %all-gather.20.cloned.1.call-done = bf16[1024,2048]{1,0:T(8,128)(2,1)} async-done(((bf16[512,2048]{1,0:T(8,128)(2,1)}), bf16[1024,2048]{1,0:T(8,128)(2,1)}) %all-gather.20.cloned.1.call-update) | async-done | bytes 4194320 | tf_op jit(solution)/shard_map/all_gather | solution.py:50
  684.5 12.0 %fusion.81 = f32[1024,1536]{1,0:T(8,128)} fusion(bf16[1024,2048]{1,0:T(8,128)(2,1)} %all-gather.20.cloned.1.call-done, bf16[2048,1536]{1,0:T(8,128)(2,1)} %all-gather.22.cloned.1.call-done), kind=kOutput, calls=%fused_computation.177 | convolution fusion | flops 6442450944 | bytes 16777216 | tf_op jit(solution)/shard_map/dot_general | solution.py:53
  696.5 51.7 %all-gather.24.cloned.1.call-done = bf16[2048,1536]{1,0:T(8,128)(2,1)} async-done(((bf16[128,1536]{1,0:T(8,128)(2,1)}), bf16[2048,1536]{1,0:T(8,128)(2,1)}) %all-gather.24.cloned.1.call-update) | async-done | bytes 6291472 | tf_op jit(solution)/shard_map/all_gather | solution.py:115
  748.2 62.4 %all-gather.26.cloned.1.call-done = bf16[2048,1536]{1,0:T(8,128)(2,1)} async-done(((bf16[128,1536]{1,0:T(8,128)(2,1)}), bf16[2048,1536]{1,0:T(8,128)(2,1)}) %all-gather.26.cloned.1.call-update) | async-done | bytes 6291472 | tf_op jit(solution)/shard_map/all_gather | solution.py:116
  810.7 21.0 %convolution_convert_fusion = bf16[1024,2048]{1,0:T(8,128)(2,1)} fusion(bf16[2048,1536]{1,0:T(8,128)(2,1)} %all-gather.26.cloned.1.call-done, f32[1024,1536]{1,0:T(8,128)} %fusion.81, bf16[1024,2048]{1,0:T(8,128)(2,1)} %all-gather.20.cloned.1.call-done, bf16[2048,1536]{1,0:T(8,128)(2,1)} %all-gather.24.cloned.1.call-done), kind=kOutput, calls=%fused_computation.20 | convolution fusion | flops 12896436224 | bytes 27262976 | tf_op jit(solution)/shard_map/dot_general | solution.py:62
  831.7 53.2 %reduce-scatter.2.cloned.1.call-done = bf16[512,2048]{1,0:T(8,128)(2,1)} async-done(((bf16[1024,2048]{1,0:T(8,128)(2,1)}), bf16[512,2048]{1,0:T(8,128)(2,1)}) %reduce-scatter.2.cloned.1.call-update) | async-done | bytes 2097168 | tf_op jit(solution)/shard_map/reduce_scatter | solution.py:61
  887.1 4.1 fusion.9
  (326 shorter events, 198.4 us)
Async XLA Ops:
  6.5 3.6 copy-start
  6.5 3.6 copy-start.29
  6.5 47.2 %all-gather.16.cloned.1.call-start = ((), (), s32[]{:S(2)}) async-start(), calls=%async_computation.5 | async-start | bytes 2228224 | tf_op jit(solution)/shard_map/all_gather | solution.py:91
  7.3 88.8 %all-gather.14.cloned.1.call-start = ((), (), s32[]{:S(2)}) async-start(), calls=%async_computation.4 | async-start | bytes 2228224 | tf_op jit(solution)/shard_map/all_gather | solution.py:89
  8.0 145.1 %all-gather.10.cloned.1.call-start = ((), (), s32[]{:S(2)}) async-start(), calls=%async_computation.2 | async-start | bytes 6291456 | tf_op jit(solution)/shard_map/all_gather | solution.py:50
  12.0 42.3 %copy-start.25 = (bf16[4,512]{1,0:T(4,128)(2,1)S(1)}, bf16[4,512]{1,0:T(4,128)(2,1)}, u32[]{:S(2)}) copy-start(bf16[4,512]{1,0:T(4,128)(2,1)} %param.22) | copy-start | bytes 12292
  12.0 42.4 %copy-start.44 = (f32[2,512]{1,0:T(2,128)S(1)}, f32[2,512]{1,0:T(2,128)}, u32[]{:S(2)}) copy-start(f32[2,512]{1,0:T(2,128)} %param.25) | copy-start | bytes 12292
  12.1 579.1 %all-gather.12.cloned.1.call-start = ((), (), s32[]{:S(2)}) async-start(), calls=%async_computation.3 | async-start | bytes 2228224 | tf_op jit(solution)/shard_map/all_gather | solution.py:90
  12.6 605.5 %all-gather.18.cloned.1.call-start = ((), (), s32[]{:S(2)}) async-start(), calls=%async_computation.6 | async-start | bytes 6291456 | tf_op jit(solution)/shard_map/all_gather | solution.py:93
  53.7 575.4 %all-gather.22.cloned.1.call-start = ((), (), s32[]{:S(2)}) async-start(), calls=%async_computation.8 | async-start | bytes 6684672 | tf_op jit(solution)/shard_map/all_gather | solution.py:114
  54.3 630.2 %all-gather.20.cloned.1.call-start = ((), (), s32[]{:S(2)}) async-start(), calls=%async_computation.7 | async-start | bytes 6291456 | tf_op jit(solution)/shard_map/all_gather | solution.py:50
  54.4 115.7 %copy-start.18 = (f32[1,512]{1,0:T(1,128)}, f32[1,512]{1,0:T(1,128)S(1)}, u32[]{:S(2)}) copy-start(f32[1,512]{1,0:T(1,128)S(1)} %get-tuple-element.53) | copy-start | bytes 6148
  54.4 115.7 %copy-start.19 = (f32[1,512]{1,0:T(1,128)}, f32[1,512]{1,0:T(1,128)S(1)}, u32[]{:S(2)}) copy-start(f32[1,512]{1,0:T(1,128)S(1)} %get-tuple-element.54) | copy-start | bytes 6148
  54.4 115.7 %copy-start.20 = (f32[1,512]{1,0:T(1,128)}, f32[1,512]{1,0:T(1,128)S(1)}, u32[]{:S(2)}) copy-start(f32[1,512]{1,0:T(1,128)S(1)} %get-tuple-element.55) | copy-start | bytes 6148
  54.4 115.7 %copy-start.21 = (f32[1,512]{1,0:T(1,128)}, f32[1,512]{1,0:T(1,128)S(1)}, u32[]{:S(2)}) copy-start(f32[1,512]{1,0:T(1,128)S(1)} %get-tuple-element.56) | copy-start | bytes 6148
  158.3 3.3 copy-start.1
  158.3 1.1 copy-start.45
  161.5 3.4 copy-start.46
  286.1 3.4 copy-start.5
  286.1 3.4 copy-start.47
  421.1 42.9 %copy-start.7 = (f32[64,512]{1,0:T(8,128)S(1)}, f32[64,512]{1,0:T(8,128)}, u32[]{:S(2)}) copy-start(f32[64,512]{1,0:T(8,128)} %get-tuple-element.26) | copy-start | bytes 393220
  427.4 38.8 %copy-start.6 = (f32[128,512]{1,0:T(8,128)S(1)}, f32[128,512]{1,0:T(8,128)}, u32[]{:S(2)}) copy-start(f32[128,512]{1,0:T(8,128)} %get-tuple-element.22) | copy-start | bytes 786436
  427.4 45.9 %copy-start.4 = (f32[512,512]{1,0:T(8,128)S(1)}, f32[512,512]{1,0:T(8,128)}, u32[]{:S(2)}) copy-start(f32[512,512]{1,0:T(8,128)} %get-tuple-element.14) | copy-start | bytes 3145732
  479.6 14.1 %copy-start.24 = (f32[2,512]{1,0:T(2,128)S(1)}, f32[2,512]{1,0:T(2,128)}, u32[]{:S(2)}) copy-start(f32[2,512]{1,0:T(2,128)} %slice.562) | copy-start | bytes 12292
  479.7 14.1 %copy-start.26 = (f32[2,512]{1,0:T(2,128)S(1)}, f32[2,512]{1,0:T(2,128)}, u32[]{:S(2)}) copy-start(f32[2,512]{1,0:T(2,128)} %slice.563) | copy-start | bytes 12292
  479.7 14.1 %copy-start.27 = (f32[2,512]{1,0:T(2,128)S(1)}, f32[2,512]{1,0:T(2,128)}, u32[]{:S(2)}) copy-start(f32[2,512]{1,0:T(2,128)} %slice.564) | copy-start | bytes 12292
  479.7 14.2 %copy-start.28 = (f32[2,512]{1,0:T(2,128)S(1)}, f32[2,512]{1,0:T(2,128)}, u32[]{:S(2)}) copy-start(f32[2,512]{1,0:T(2,128)} %slice.566) | copy-start | bytes 12292
  479.7 14.2 %copy-start.17 = (f32[4,512]{1,0:T(4,128)S(1)}, f32[4,512]{1,0:T(4,128)}, u32[]{:S(2)}) copy-start(f32[4,512]{1,0:T(4,128)} %get-tuple-element.42) | copy-start | bytes 24580
  479.7 15.0 %copy-start.22 = (f32[3,512]{1,0:T(4,128)S(1)}, f32[3,512]{1,0:T(4,128)}, u32[]{:S(2)}) copy-start(f32[3,512]{1,0:T(4,128)} %slice.555) | copy-start | bytes 18436
  479.7 15.0 %copy-start.23 = (f32[3,512]{1,0:T(4,128)S(1)}, f32[3,512]{1,0:T(4,128)}, u32[]{:S(2)}) copy-start(f32[3,512]{1,0:T(4,128)} %slice.572) | copy-start | bytes 18436
  479.7 15.0 %copy-start.43 = (f32[1,512]{1,0:T(1,128)S(1)}, f32[1,512]{1,0:T(1,128)}, u32[]{:S(2)}) copy-start(f32[1,512]{1,0:T(1,128)} %slice.676) | copy-start | bytes 6148
  479.7 15.1 %copy-start.15 = (f32[7,512]{1,0:T(8,128)S(1)}, f32[7,512]{1,0:T(8,128)}, u32[]{:S(2)}) copy-start(f32[7,512]{1,0:T(8,128)} %slice.549) | copy-start | bytes 43012
  479.7 15.1 %copy-start.16 = (f32[7,512]{1,0:T(8,128)S(1)}, f32[7,512]{1,0:T(8,128)}, u32[]{:S(2)}) copy-start(f32[7,512]{1,0:T(8,128)} %slice.574) | copy-start | bytes 43012
  479.7 15.1 %copy-start.42 = (f32[1,512]{1,0:T(1,128)S(1)}, f32[1,512]{1,0:T(1,128)}, u32[]{:S(2)}) copy-start(f32[1,512]{1,0:T(1,128)} %slice.675) | copy-start | bytes 6148
  479.7 15.1 %copy-start.13 = (f32[15,512]{1,0:T(8,128)S(1)}, f32[15,512]{1,0:T(8,128)}, u32[]{:S(2)}) copy-start(f32[15,512]{1,0:T(8,128)} %slice.543) | copy-start | bytes 92164
  479.7 15.1 %copy-start.14 = (f32[15,512]{1,0:T(8,128)S(1)}, f32[15,512]{1,0:T(8,128)}, u32[]{:S(2)}) copy-start(f32[15,512]{1,0:T(8,128)} %slice.576) | copy-start | bytes 92164
  479.7 15.2 %copy-start.41 = (f32[1,512]{1,0:T(1,128)S(1)}, f32[1,512]{1,0:T(1,128)}, u32[]{:S(2)}) copy-start(f32[1,512]{1,0:T(1,128)} %slice.674) | copy-start | bytes 6148
  486.1 8.9 copy-start.11
  486.1 8.9 copy-start.12
  486.1 9.0 copy-start.40
  486.1 9.7 %copy-start.9 = (f32[63,512]{1,0:T(8,128)S(1)}, f32[63,512]{1,0:T(8,128)}, u32[]{:S(2)}) copy-start(f32[63,512]{1,0:T(8,128)} %slice.531) | copy-start | bytes 387076
  486.1 9.7 %copy-start.10 = (f32[63,512]{1,0:T(8,128)S(1)}, f32[63,512]{1,0:T(8,128)}, u32[]{:S(2)}) copy-start(f32[63,512]{1,0:T(8,128)} %slice.580) | copy-start | bytes 387076
  486.1 9.7 %copy-start.39 = (f32[1,512]{1,0:T(1,128)S(1)}, f32[1,512]{1,0:T(1,128)}, u32[]{:S(2)}) copy-start(f32[1,512]{1,0:T(1,128)} %slice.672) | copy-start | bytes 6148
  502.3 2.4 copy-start.38
  523.3 2.3 copy-start.37
  530.7 8.3 copy-start.8
  530.7 8.4 copy-start.36
  539.0 3.0 copy-start.35
  542.1 2.3 copy-start.34
  563.0 2.3 copy-start.33
  618.1 5.0 copy-start.30
  623.1 2.5 copy-start.31
  624.2 1.4 copy-start.2
  627.6 120.7 %all-gather.24.cloned.1.call-start = ((), (), s32[]{:S(2)}) async-start(), calls=%async_computation.9 | async-start | bytes 6684672 | tf_op jit(solution)/shard_map/all_gather | solution.py:115
  628.3 182.4 %all-gather.26.cloned.1.call-start = ((), (), s32[]{:S(2)}) async-start(), calls=%async_computation.10 | async-start | bytes 6684672 | tf_op jit(solution)/shard_map/all_gather | solution.py:116
  629.0 255.9 %reduce-scatter.2.cloned.1.call-start = ((), (), s32[]{:S(2)}) async-start(), calls=%async_computation.11 | async-start | bytes 6291456 | tf_op jit(solution)/shard_map/reduce_scatter | solution.py:61
  831.7 55.3 %copy-start.32 = (f32[2048]{0:T(1024)S(1)}, f32[2048]{0:T(1024)}, u32[]{:S(2)}) copy-start(f32[2048]{0:T(1024)} %param.19) | copy-start | bytes 24580
  831.7 55.3 %copy-start.3 = (bf16[512,2048]{1,0:T(8,128)(2,1)S(1)}, bf16[512,2048]{1,0:T(8,128)(2,1)}, u32[]{:S(2)}) copy-start(bf16[512,2048]{1,0:T(8,128)(2,1)} %copy-done.2) | copy-start | bytes 6291460
Sparse Core Ops, SparseCore 0:
  9.5 44.1 all-gather.15
  55.9 40.1 all-gather.13
  97.6 55.4 all-gather.9
  155.1 41.4 all-gather.11
  198.0 55.4 all-gather.17
  255.6 61.3 all-gather.21
  627.7 56.7 all-gather.19
  686.8 61.3 all-gather.23
  750.5 60.0 all-gather.25
  831.8 53.0 reduce-scatter.1
where the time goes:
time: 914 us; the launch traced here: 898 us
  waiting for transfers between devices  366 us (40%)
  local copies, waits for them, and re-layouts  335 us (37%)
  other arithmetic  103 us (11%)
  matrix products  61.6 us (7%)
  blocking collectives  17 us (2%)
  between operations  14.8 us (2%)
    slice x120, local copies, waits for them, and re-layouts, recurrence(): unused_decay, states = lax.associative_scan(combine, (retain, feed), axis=0)  242 us
    all_gather x2, waiting for transfers between devices, gathered_product(): row_piece = lax.all_gather(normed_rows, 'tp', axis=0, tiled=True)  112 us
    all_gather x1, waiting for transfers between devices, per_device(): lax.all_gather(down_weight_t, 'fs', axis=0, tiled=True)  62.4 us
    reduce_scatter x1, waiting for transfers between devices, summed_rows(): lax.psum_scatter(lax.dot_general(hidden, weight_t, (((1,), (1,)), ((), ()...  53.2 us
    all_gather x1, waiting for transfers between devices, per_device(): lax.all_gather(w_up, 'fs', axis=0, tiled=True)  51.7 us
    pad x36, local copies, waits for them, and re-layouts, recurrence(): unused_decay, states = lax.associative_scan(combine, (retain, feed), axis=0)  44.9 us
    all_gather x1, waiting for transfers between devices, per_device(): lax.all_gather(w_branch, 'fs', axis=0, tiled=True)  41.1 us
    all_gather x1, waiting for transfers between devices, per_device(): lax.all_gather(out_weight_t, 'fs', axis=0, tiled=True)  41 us
  transfers between devices with their start and end apart: 10, of which 7 were waited for; matrix products, arithmetic and copies ran while one was open for 52% of the time, Pallas kernels for 0%

commit v1 on v0

v1 whole, which is shorter than its diff:
```python
import functools

import jax
import jax.numpy as jnp
from jax import lax
from jax.experimental import pallas as pl
from jax.experimental.pallas import tpu as pltpu
from jax.sharding import PartitionSpec as P

EPS = 1e-06
SEGMENTS = 8
VMEM_BYTES = 60 * 1024 * 1024


def normed(values, gain):
    factor = lax.rsqrt(jnp.mean(values * values, axis=-1, keepdims=True) + EPS)
    return values * factor * gain


def one_minus_exp(y, exp_y):
    series = 1.0 + y * (1.0 / 8.0)
    for order in (7, 6, 5, 4, 3, 2):
        series = 1.0 + y * (1.0 / order) * series
    return jnp.where(y > -0.5, -y * series, 1.0 - exp_y)


def mixer_kernel(
    x_ref, wb_ref, wg_ref, conv_ref, gates_ref, coef_ref, out_ref, pad, gel, a0, u0, a1, u1
):
    length, width = out_ref.shape
    group = gates_ref.shape[1]
    rows = 256
    pad[0:8, :] = jnp.zeros((8, width), jnp.float32)
    pad[8 + length : 16 + length, :] = jnp.zeros((8, width), jnp.float32)
    for start in range(0, length, rows):
        piece = x_ref[start : start + rows, :]
        branch = jnp.dot(piece, wb_ref[...], preferred_element_type=jnp.float32)
        pad[8 + start : 8 + start + rows, :] = branch.astype(jnp.bfloat16).astype(jnp.float32)
        gelu_in = jnp.dot(piece, wg_ref[...], preferred_element_type=jnp.float32)
        gel[start : start + rows, :] = jax.nn.gelu(
            gelu_in.astype(jnp.bfloat16).astype(jnp.float32)
        )

    for part in range(width // group):
        cols = slice(part * group, (part + 1) * group)
        taps = conv_ref[:, cols].astype(jnp.float32)
        coef = coef_ref[:, cols]
        for start in range(0, length, rows):
            summed = taps[0:1] * pad[6 + start : 6 + start + rows, cols]
            for j in range(1, 4):
                summed = summed + taps[j : j + 1] * pad[6 + j + start : 6 + j + start + rows, cols]
            conv = summed.astype(jnp.bfloat16)
            wide = conv.astype(jnp.float32)
            for d, (a_ref, u_ref) in enumerate(((a0, u0), (a1, u1))):
                gate = jnp.dot(
                    conv,
                    gates_ref[part, :, 2 * d * group : 2 * (d + 1) * group],
                    preferred_element_type=jnp.float32,
                )
                rate = jax.nn.sigmoid(gate[:, :group])
                inflow = jax.nn.sigmoid(gate[:, group:])
                log_retain = rate * coef[d : d + 1]
                retain = jnp.exp(log_retain)
                left = one_minus_exp(2.0 * log_retain, retain * retain)
                a_ref[part, start : start + rows, :] = retain
                u_ref[part, start : start + rows, :] = jnp.sqrt(left) * inflow * wide

    steps = length // SEGMENTS

    def step(t, carry):
        out = []
        for (state, decayed), (a_ref, u_ref), at in (
            (carry[0], (a0, u0), t),
            (carry[1], (a1, u1), steps - 1 - t),
        ):
            where = pl.ds(at, SEGMENTS, stride=steps)
            nstate, ndecayed = [], []
            for c in range(n):
                retain = a_ref[c, where, :]
                h = retain * state[c] + u_ref[c, where, :]
                p = retain * decayed[c]
                u_ref[c, where, :] = h
                a_ref[c, where, :] = p
                nstate.append(h)
                ndecayed.append(p)
            out.append((tuple(nstate), tuple(ndecayed)))
        return tuple(out)

    n = width // group
    zero = tuple(jnp.zeros((SEGMENTS, group), jnp.float32) for c in range(n))
    one = tuple(jnp.ones((SEGMENTS, group), jnp.float32) for c in range(n))
    ended = lax.fori_loop(0, steps, step, ((zero, one), (zero, one)), unroll=8)
    for c in range(n):
        lanes = slice(c * group, (c + 1) * group)
        blank = jnp.zeros((1, group), jnp.float32)
        entry = [[None] * SEGMENTS, [None] * SEGMENTS]
        for d, order in ((0, range(SEGMENTS)), (1, range(SEGMENTS - 1, -1, -1))):
            carry = blank
            for s in order:
                entry[d][s] = carry
                carry = ended[d][0][c][s : s + 1] + ended[d][1][c][s : s + 1] * carry
        for s in range(SEGMENTS):
            span = slice(s * steps, (s + 1) * steps)
            forward = u0[c, span, :] + a0[c, span, :] * entry[0][s]
            backward = u1[c, span, :] + a1[c, span, :] * entry[1][s]
            out_ref[span, lanes] = (gel[span, lanes] * (forward + backward)).astype(jnp.bfloat16)


def mixer(x, weights, conv_weight, w_rec, w_inp, decay):
    length, model = x.shape
    channels = conv_weight.shape[1]
    group = w_rec.shape[2]
    width = min(256, channels)
    count = channels // width
    gates = jnp.concatenate([w_rec[0], w_inp[0], w_rec[1], w_inp[1]], axis=-1)
    coef = -8.0 * jax.nn.softplus(-decay)
    f32 = functools.partial(pltpu.VMEM, dtype=jnp.float32)
    return pl.pallas_call(
        mixer_kernel,
        grid=(count,),
        out_shape=jax.ShapeDtypeStruct((length, channels), jnp.bfloat16),
        in_specs=[
            pl.BlockSpec((length, model), lambda j: (0, 0)),
            pl.BlockSpec((model, width), lambda j: (0, j)),
            pl.BlockSpec((model, width), lambda j: (0, count + j)),
            pl.BlockSpec((4, width), lambda j: (0, j)),
            pl.BlockSpec((width // group, group, 4 * group), lambda j: (j, 0, 0)),
            pl.BlockSpec((2, width), lambda j: (0, j)),
        ],
        out_specs=pl.BlockSpec((length, width), lambda j: (0, j)),
        scratch_shapes=[f32((length + 16, width)), f32((length, width))]
        + [f32((width // group, length, group)) for i in range(4)],
        compiler_params=pltpu.CompilerParams(vmem_limit_bytes=VMEM_BYTES),
        cost_estimate=pl.CostEstimate(
            flops=4 * length * model * channels + 16 * length * group * channels * 8,
            bytes_accessed=2 * (length * model + 2 * model * channels + length * channels),
            transcendentals=12 * length * channels,
        ),
    )(x, weights, weights, conv_weight, gates, coef)


def ffn_kernel(x_ref, gate_ref, up_ref, down_ref, out_ref, total):
    step = pl.program_id(0)
    gate = jnp.dot(x_ref[...], gate_ref[...], preferred_element_type=jnp.float32)
    up = jnp.dot(x_ref[...], up_ref[...], preferred_element_type=jnp.float32)
    hidden = (jax.nn.silu(gate) * up).astype(jnp.bfloat16)
    partial = lax.dot_general(
        hidden, down_ref[...], (((1,), (1,)), ((), ())), preferred_element_type=jnp.float32
    )

    @pl.when(step == 0)
    def _():
        total[...] = partial

    @pl.when(step > 0)
    def _():
        total[...] += partial

    @pl.when(step == pl.num_programs(0) - 1)
    def _():
        out_ref[...] = total[...].astype(jnp.bfloat16)


def ffn(x, weights):
    rows, model = x.shape
    units = weights.shape[1] // 3
    width = 256 if units % 256 == 0 else 128
    count = units // width
    return pl.pallas_call(
        ffn_kernel,
        grid=(count,),
        out_shape=jax.ShapeDtypeStruct((rows, model), jnp.bfloat16),
        in_specs=[
            pl.BlockSpec((rows, model), lambda j: (0, 0)),
            pl.BlockSpec((model, width), lambda j: (0, j)),
            pl.BlockSpec((model, width), lambda j: (0, count + j)),
            pl.BlockSpec((model, width), lambda j: (0, 2 * count + j)),
        ],
        out_specs=pl.BlockSpec((rows, model), lambda j: (0, 0)),
        scratch_shapes=[pltpu.VMEM((rows, model), jnp.float32)],
        compiler_params=pltpu.CompilerParams(vmem_limit_bytes=VMEM_BYTES),
        cost_estimate=pl.CostEstimate(
            flops=6 * rows * model * units,
            bytes_accessed=2 * (2 * rows * model + 3 * model * units),
            transcendentals=rows * units,
        ),
    )(x, weights, weights, weights)


def swap(values):
    return lax.ppermute(values, "tp", [(0, 1), (1, 0)])


def matmul_t(rows, weight_t):
    return lax.dot_general(
        rows, weight_t, (((1,), (1,)), ((), ())), preferred_element_type=jnp.float32
    )


def per_device(
    pair,
    tokens,
    pre_mix_gain,
    post_mix_gain,
    pre_ffn_gain,
    post_ffn_gain,
    w_branch,
    w_gelu,
    conv_weight,
    w_rec,
    w_inp,
    decay,
    out_weight_t,
    w_gate,
    w_up,
    down_weight_t,
):
    own_rows = tokens.shape[0]
    channels = conv_weight.shape[1]
    place = lax.axis_index("tp")
    parts = [w_branch, w_gelu, out_weight_t]
    if pair:
        parts.append(swap(out_weight_t))
    mix_all = lax.all_gather(jnp.concatenate(parts, axis=1), "fs", axis=0, tiled=True)
    ffn_all = lax.all_gather(
        jnp.concatenate([w_gate, w_up, down_weight_t], axis=1), "fs", axis=0, tiled=True
    )
    stream = tokens.astype(jnp.float32)
    normed_in = normed(stream, pre_mix_gain).astype(jnp.bfloat16)
    if pair:
        other = swap(normed_in)
        first = jnp.where(place == 0, normed_in, other)
        second = jnp.where(place == 0, other, normed_in)
        sequence = jnp.concatenate([first, second], axis=0)
    else:
        sequence = lax.all_gather(normed_in, "tp", axis=0, tiled=True)
    hidden = mixer(sequence, mix_all, conv_weight, w_rec, w_inp, decay)
    out_own = mix_all[:, 2 * channels : 3 * channels]
    if pair:
        away = lax.dynamic_slice_in_dim(hidden, (1 - place) * own_rows, own_rows, 0)
        kept = lax.dynamic_slice_in_dim(hidden, place * own_rows, own_rows, 0)
        came = swap(away)
        mixer_sum = matmul_t(kept, out_own) + matmul_t(came, mix_all[:, 3 * channels :])
    else:
        own_hidden = lax.all_to_all(hidden, "tp", split_axis=0, concat_axis=1, tiled=True)
        out_whole = lax.all_gather(out_own, "tp", axis=1, tiled=True)
        mixer_sum = matmul_t(own_hidden, out_whole)
    residual = (stream + normed(mixer_sum, post_mix_gain)).astype(jnp.bfloat16)
    middle = residual.astype(jnp.float32)
    normed_mid = normed(middle, pre_ffn_gain).astype(jnp.bfloat16)
    if pair:
        pieces = 2
        size = own_rows // pieces
        sums = []
        away_rows = [swap(normed_mid[i * size : (i + 1) * size]) for i in range(pieces)]
        back = [swap(ffn(rows, ffn_all)) for rows in away_rows]
        own_part = ffn(normed_mid, ffn_all).astype(jnp.float32)
        ffn_sum = own_part + jnp.concatenate(back, axis=0).astype(jnp.float32)
    else:
        all_mid = lax.all_gather(normed_mid, "tp", axis=0, tiled=True)
        ffn_sum = lax.psum_scatter(
            ffn(all_mid, ffn_all), "tp", scatter_dimension=0, tiled=True
        ).astype(jnp.float32)
    return (middle + normed(ffn_sum, post_ffn_gain)).astype(jnp.bfloat16)


def solution(mesh):
    return jax.shard_map(
        functools.partial(per_device, mesh.shape["tp"] == 2),
        mesh=mesh,
        in_specs=(
            P(("fs", "tp"), None),
            P(),
            P(),
            P(),
            P(),
            P("fs", "tp"),
            P("fs", "tp"),
            P(None, "tp"),
            P(None, "tp", None, None),
            P(None, "tp", None, None),
            P(None, "tp"),
            P("fs", "tp"),
            P("fs", "tp"),
            P("fs", "tp"),
            P("fs", "tp"),
        ),
        out_specs=P(("fs", "tp"), None),
        check_vma=False,
    )
```

time: 914 us -> 264 us (0.29); the launches traced: 898 us -> 263 us
  local copies, waits for them, and re-layouts: 335 us -> 2.58 us
  waiting for transfers between devices: 366 us -> 139 us
  other arithmetic: 103 us -> 21 us
  Pallas kernels: 0 us -> 70.7 us
  matrix products: 61.6 us -> 5.85 us
  blocking collectives: 17 us -> 0 us
  starting transfers between devices: 0.35 us -> 10.3 us
    all_gather x9 -> x2, waiting for transfers between devices: 309 us -> 39.5 us  [the longest x1 21.4 us: per_device(): lax.all_gather(jnp.concatenate([w_gate, w_up, down_weight_t], axis=1), 'f...]
    slice x121 -> x1, local copies, waits for them, and re-layouts: 242 us -> 1.4 us  [per_device(): normed_mid[i * size:(i + 1) * size]]
    ppermute x0 -> x7, waiting for transfers between devices: none -> 99.6 us  [swap(): return lax.ppermute(values, 'tp', [(0, 1), (1, 0)])]
    pallas_call x0 -> x4, Pallas kernels: none -> 70.7 us  [the longest x3 43.3 us: ffn(): pl.pallas_call(ffn_kernel, grid=(count,), out_shape=jax.ShapeDtypeStruct(...]
    dot_general x9 -> x2, matrix products: 61.6 us -> 5.85 us  [matmul_t(): lax.dot_general(rows, weight_t, (((1,), (1,)), ((), ())), preferred_eleme...]
    reduce_scatter x1 -> x0, waiting for transfers between devices: 53.2 us -> none  [summed_rows(): lax.psum_scatter(lax.dot_general(hidden, weight_t, (((1,), (1,)), ((), ()...]
    pad x36 -> x0, local copies, waits for them, and re-layouts: 44.9 us -> none  [recurrence(): unused_decay, states = lax.associative_scan(combine, (retain, feed), axis=0)]
    mul x17 -> x1, other arithmetic: 33.5 us -> 0.61 us  [mixer(): coef = -8.0 * jax.nn.softplus(-decay)]
  transfers between devices with their start and end apart: 10 -> 9, of which waited for: 7 -> 7; matrix products, arithmetic and copies ran while one was open for 52% -> 8% of each run, Pallas kernels for 0% -> 27%
where the time goes in v1:
time: 264 us; the launch traced here: 263 us
  waiting for transfers between devices  139 us (53%)
  Pallas kernels  70.7 us (27%)
  other arithmetic  21 us (8%)
  between operations  13.6 us (5%)
  starting transfers between devices  10.3 us (4%)
  matrix products  5.85 us (2%)
    ppermute x7, waiting for transfers between devices, swap(): return lax.ppermute(values, 'tp', [(0, 1), (1, 0)])  99.6 us
    pallas_call x3, Pallas kernels, ffn(): pl.pallas_call(ffn_kernel, grid=(count,), out_shape=jax.ShapeDtypeStruct(...  43.3 us
    pallas_call x1, Pallas kernels, mixer(): pl.pallas_call(mixer_kernel, grid=(count,), out_shape=jax.ShapeDtypeStruc...  27.4 us
    all_gather x1, waiting for transfers between devices, per_device(): lax.all_gather(jnp.concatenate([w_gate, w_up, down_weight_t], axis=1), 'f...  21.4 us
    all_gather x1, waiting for transfers between devices, per_device(): lax.all_gather(jnp.concatenate(parts, axis=1), 'fs', axis=0, tiled=True)  18.1 us
    ppermute x7, starting transfers between devices, swap(): return lax.ppermute(values, 'tp', [(0, 1), (1, 0)])  10.3 us
    dot_general x2, matrix products, matmul_t(): lax.dot_general(rows, weight_t, (((1,), (1,)), ((), ())), preferred_eleme...  5.85 us
  transfers between devices with their start and end apart: 9, of which 7 were waited for; matrix products, arithmetic and copies ran while one was open for 8% of the time, Pallas kernels for 27%

profile of v1, /device:TPU:0, one launch (start us, length us, event | category | flops | bytes accessed | tf_op | source)
XLA Modules:
  0.0 263.1 jit_solution(9239097312352929329)
XLA Ops:
  6.5 0.0 copy-start
  6.5 0.0 copy-start.9
  6.5 0.0 all-gather.3.cloned.1.call-start
  6.5 3.0 %collective-permute-start.1 = (bf16[128,512]{1,0:T(8,128)(2,1)}, bf16[128,512]{1,0:T(8,128)(2,1)S(1)}, u32[]{:S(2)}, u32[]{:S(2)}) collective-permute-start(bf16[128,512]{1,0:T(8,128)(2,1)} %param.26), channel_id=1, source_target_pairs={{0,1},{1,0},{2,3},{3,2},{4,5},{5,4},{6,7},{7,6},{8,9},{9,8},{10,11... | collective-permute-start | bytes 393224 | tf_op jit(solution)/shard_map/ppermute | solution.py:191
  9.5 3.7 %collective-permute-done.1 = bf16[128,512]{1,0:T(8,128)(2,1)S(1)} collective-permute-done((bf16[128,512]{1,0:T(8,128)(2,1)}, bf16[128,512]{1,0:T(8,128)(2,1)S(1)}, u32[]{:S(2)}, u32[]{:S(2)}) %collective-permute-start.1) | collective-permute-done | bytes 131104 | tf_op jit(solution)/shard_map/ppermute | solution.py:191
  13.2 1.9 pad_maximum_fusion.3
  15.1 0.0 all-gather.3.cloned.1.call-update
  15.1 0.0 all-gather.5.cloned.1.call-start
  15.2 2.4 pad_maximum_fusion.2
  17.6 0.0 copy-start.7
  17.6 0.0 copy-start.8
  17.6 0.0 all-gather.5.cloned.1.call-update
  17.6 0.0 copy-done
  17.6 0.0 copy-start.13
  17.6 0.5 fusion
  18.1 0.0 copy-done.9
  18.1 1.9 fusion.2
  20.0 1.7 collective-permute-start
  21.7 0.0 copy-done.7
  21.7 0.0 copy-done.8
  21.8 0.9 pad_maximum_fusion.4.gates_ref
  22.7 0.0 copy-done.13
  22.7 0.6 fusion.12.coef_ref
  23.3 43.8 %collective-permute-done = bf16[512,2048]{1,0:T(8,128)(2,1)} collective-permute-done((bf16[512,2048]{1,0:T(8,128)(2,1)}, bf16[512,2048]{1,0:T(8,128)(2,1)}, u32[]{:S(2)}, u32[]{:S(2)}) %collective-permute-start) | collective-permute-done | bytes 2097184 | tf_op jit(solution)/shard_map/ppermute | solution.py:191
  67.1 3.2 %broadcast_select_fusion.1 = (bf16[512,2048]{1,0:T(8,128)(2,1)S(1)}, bf16[512,2048]{1,0:T(8,128)(2,1)S(1)}) fusion(bf16[512,2048]{1,0:T(8,128)(2,1)} %collective-permute-done, pred[]{:T(512)S(6)} %eq.4, f32[2048]{0:T(1024)S(1)} %copy-done.9, f32[512]{0:T(512)S(1)} %add_rsqrt_fusion.3, bf16[512,2048]{1,0:T(8,128)(2,1)S(1)} %copy-done), kind=kLoop, calls=%fused_computation.24 | loop fusion | flops 6291456 | bytes 8398849 | tf_op jit(solution)/shard_map/jit(_where)/select_n | solution.py:232
  70.3 2.7 %pad_maximum_fusion.x_ref = bf16[1024,2048]{1,0:T(8,128)(2,1)} fusion(bf16[512,2048]{1,0:T(8,128)(2,1)S(1)} %get-tuple-element.8, bf16[512,2048]{1,0:T(8,128)(2,1)S(1)} %get-tuple-element.7), kind=kLoop, calls=%fused_computation.14 | loop fusion | flops 8388608 | bytes 8388608 | tf_op jit(solution)/shard_map/concatenate | solution.py:234
  73.0 18.1 %all-gather.3.cloned.1.call-done.wb_ref.wg_ref = bf16[2048,2048]{1,0:T(8,128)(2,1)} async-done(((bf16[128,2048]{1,0:T(8,128)(2,1)}), bf16[2048,2048]{1,0:T(8,128)(2,1)}) %all-gather.3.cloned.1.call-update) | async-done | bytes 8388624 | tf_op jit(solution)/shard_map/all_gather | solution.py:224
  91.1 27.4 %shard_map.145 = bf16[1024,512]{1,0:T(8,128)(2,1)} custom-call(bf16[1024,2048]{1,0:T(8,128)(2,1)} %pad_maximum_fusion.x_ref, bf16[2048,2048]{1,0:T(8,128)(2,1)} %all-gather.3.cloned.1.call-done.wb_ref.wg_ref, bf16[2048,2048]{1,0:T(8,128)(2,1)} %all-gather.3.cloned.1.call-done.wb_ref.wg_ref, bf16[4,512]{1,0:T(4,128)(2,1)} %conv_ref.1, ...), custom_call_target="tpu_custom_call" | custom-call | flops 12884901888 | bytes 9437184 | tf_op jit(solution)/shard_map/pallas_call | solution.py:118
  118.5 1.1 constant_dynamic-slice_fusion
  119.6 1.5 collective-permute-start.2
  121.1 0.0 copy-start.6
  121.1 12.7 %collective-permute-done.2 = bf16[512,512]{1,0:T(8,128)(2,1)S(1)} collective-permute-done((bf16[512,512]{1,0:T(8,128)(2,1)S(1)}, bf16[512,512]{1,0:T(8,128)(2,1)S(1)}, u32[]{:S(2)}, u32[]{:S(2)}) %collective-permute-start.2) | collective-permute-done | bytes 524320 | tf_op jit(solution)/shard_map/ppermute | solution.py:191
  133.8 2.9 %fusion.8 = f32[512,2048]{1,0:T(8,128)S(1)} fusion(bf16[512,512]{1,0:T(8,128)(2,1)S(1)} %collective-permute-done.2, bf16[2048,2048]{1,0:T(8,128)(2,1)} %all-gather.3.cloned.1.call-done.wb_ref.wg_ref), kind=kOutput, calls=%fused_computation.19 | convolution fusion | flops 1073741824 | bytes 6815744 | tf_op jit(solution)/shard_map/dot_general | solution.py:195
  136.7 0.0 copy-done.6
  136.7 0.0 copy-start.10
  136.7 3.0 %multiply_reduce_fusion.1 = (f32[512]{0:T(512)S(1)}, f32[512,2048]{1,0:T(8,128)S(1)}) fusion(f32[512,2048]{1,0:T(8,128)S(1)} %fusion.8, bf16[2048,2048]{1,0:T(8,128)(2,1)} %all-gather.3.cloned.1.call-done.wb_ref.wg_ref, bf16[1024,512]{1,0:T(8,128)(2,1)S(1)} %copy-done.6, s32[]{:T(128)S(6)} %select_n.26), kind=kOutput, calls=%fused_computation.17 | convolution fusion | flops 1076887040 | bytes 11012100 | tf_op jit(solution)/shard_map/dot_general | solution.py:195
  139.7 0.0 copy-done.10
  139.7 0.0 copy-start.11
  139.7 1.1 fusion.4
  140.8 0.0 copy-start.1
  140.8 0.0 copy-done.11
  140.8 0.6 fusion.6.x_ref
  141.4 0.0 copy-start.3
  141.4 1.4 fusion.15
  142.8 0.0 copy-done.1
  142.8 1.4 collective-permute-start.3
  144.2 0.6 collective-permute-start.5
  144.8 24.0 %collective-permute-done.3.x_ref = bf16[256,2048]{1,0:T(8,128)(2,1)S(1)} collective-permute-done((bf16[256,2048]{1,0:T(8,128)(2,1)S(1)}, bf16[256,2048]{1,0:T(8,128)(2,1)S(1)}, u32[]{:S(2)}, u32[]{:S(2)}) %collective-permute-start.3) | collective-permute-done | bytes 1048608 | tf_op jit(solution)/shard_map/ppermute | solution.py:191
  168.8 21.4 %all-gather.5.cloned.1.call-done.gate_ref.up_ref.down_ref = bf16[2048,4608]{1,0:T(8,128)(2,1)} async-done(((bf16[128,4608]{1,0:T(8,128)(2,1)}), bf16[2048,4608]{1,0:T(8,128)(2,1)}) %all-gather.5.cloned.1.call-update) | async-done | bytes 18874384 | tf_op jit(solution)/shard_map/all_gather | solution.py:225
  190.2 0.0 copy-done.5
  190.2 12.7 %shard_map.147 = bf16[256,2048]{1,0:T(8,128)(2,1)} custom-call(bf16[256,2048]{1,0:T(8,128)(2,1)} %copy-done.5, bf16[2048,4608]{1,0:T(8,128)(2,1)} %all-gather.5.cloned.1.call-done.gate_ref.up_ref.down_ref, bf16[2048,4608]{1,0:T(8,128)(2,1)} %all-gather.5.cloned.1.call-done.gate_ref.up_ref.down_ref, ...), custom_call_target="tpu_custom_call" | custom-call | flops 4831838208 | bytes 20971520 | tf_op jit(solution)/shard_map/pallas_call | solution.py:169
  203.0 0.0 copy-done.3
  203.0 1.5 collective-permute-start.4
  204.4 0.0 collective-permute-done.5.x_ref
  204.4 12.8 %shard_map.148 = bf16[256,2048]{1,0:T(8,128)(2,1)} custom-call(bf16[256,2048]{1,0:T(8,128)(2,1)} %collective-permute-done.5.x_ref, bf16[2048,4608]{1,0:T(8,128)(2,1)} %all-gather.5.cloned.1.call-done.gate_ref.up_ref.down_ref, bf16[2048,4608]{1,0:T(8,128)(2,1)} %all-gather.5.cloned.1.call-done.gate_ref.up_ref.down_ref, ...), custom_call_target="tpu_custom_call" | custom-call | flops 4831838208 | bytes 20971520 | tf_op jit(solution)/shard_map/pallas_call | solution.py:169
  217.2 0.6 collective-permute-start.6
  217.8 17.7 %shard_map.146 = bf16[512,2048]{1,0:T(8,128)(2,1)} custom-call(bf16[512,2048]{1,0:T(8,128)(2,1)} %copy-done.3, bf16[2048,4608]{1,0:T(8,128)(2,1)} %all-gather.5.cloned.1.call-done.gate_ref.up_ref.down_ref, bf16[2048,4608]{1,0:T(8,128)(2,1)} %all-gather.5.cloned.1.call-done.gate_ref.up_ref.down_ref, ...), custom_call_target="tpu_custom_call" | custom-call | flops 9663676416 | bytes 23068672 | tf_op jit(solution)/shard_map/pallas_call | solution.py:169
  235.5 0.0 collective-permute-done.4
  235.5 15.4 %collective-permute-done.6 = bf16[256,2048]{1,0:T(8,128)(2,1)S(1)} collective-permute-done((bf16[256,2048]{1,0:T(8,128)(2,1)}, bf16[256,2048]{1,0:T(8,128)(2,1)S(1)}, u32[]{:S(2)}, u32[]{:S(2)}) %collective-permute-start.6) | collective-permute-done | bytes 1048608 | tf_op jit(solution)/shard_map/ppermute | solution.py:191
  251.0 2.3 multiply_reduce_fusion
  253.3 0.0 copy-done.12
  253.3 0.0 copy-done.2
  253.3 0.0 copy-done.4
  253.3 3.0 %fusion.7 = bf16[512,2048]{1,0:T(8,128)(2,1)} fusion(bf16[512,2048]{1,0:T(8,128)(2,1)S(1)} %copy-done.2, bf16[512,2048]{1,0:T(8,128)(2,1)S(1)} %copy-done.4, f32[2048]{0:T(1024)S(1)} %copy-done.12, f32[512]{0:T(512)S(1)} %add_rsqrt_fusion, bf16[256,2048]{1,0:T(8,128)(2,1)S(1)} %collective-permute-done.6, bf16[256,2048]{1,0:T(8,128)(2,1)S(1)} %collective-permute-done.4), kind=kLoop, calls=%fused_computation.13 | loop fusion | flops 11534336 | bytes 8398848 | tf_op jit(solution)/shard_map/convert_element_type | solution.py:264
  (9 shorter events, 0.1 us)
Async XLA Ops:
  6.5 11.1 %copy-start = (bf16[512,2048]{1,0:T(8,128)(2,1)S(1)}, bf16[512,2048]{1,0:T(8,128)(2,1)}, u32[]{:S(2)}) copy-start(bf16[512,2048]{1,0:T(8,128)(2,1)} %param.15) | copy-start | bytes 6291460
  6.5 11.6 %copy-start.9 = (f32[2048]{0:T(1024)S(1)}, f32[2048]{0:T(1024)}, u32[]{:S(2)}) copy-start(f32[2048]{0:T(1024)} %param.16) | copy-start | bytes 24580
  6.5 84.6 %all-gather.3.cloned.1.call-start = ((), (), s32[]{:S(2)}) async-start(), calls=%async_computation | async-start | bytes 8912896 | tf_op jit(solution)/shard_map/all_gather | solution.py:224
  6.5 6.7 %collective-permute-start.1 = (bf16[128,512]{1,0:T(8,128)(2,1)}, bf16[128,512]{1,0:T(8,128)(2,1)S(1)}, u32[]{:S(2)}, u32[]{:S(2)}) collective-permute-start(bf16[128,512]{1,0:T(8,128)(2,1)} %param.26), channel_id=1, source_target_pairs={{0,1},{1,0},{2,3},{3,2},{4,5},{5,4},{6,7},{7,6},{8,9},{9,8},{10,11... | collective-permute-start | bytes 393224 | tf_op jit(solution)/shard_map/ppermute | solution.py:191
  15.1 175.1 %all-gather.5.cloned.1.call-start = ((), (), s32[]{:S(2)}) async-start(), calls=%async_computation.1 | async-start | bytes 20054016 | tf_op jit(solution)/shard_map/all_gather | solution.py:225
  17.6 4.2 %copy-start.7 = (bf16[2,4,128,128]{3,2,1,0:T(8,128)(2,1)S(1)}, bf16[2,4,128,128]{3,2,1,0:T(8,128)(2,1)}, u32[]{:S(2)}) copy-start(bf16[2,4,128,128]{3,2,1,0:T(8,128)(2,1)} %param.24) | copy-start | bytes 786436
  17.6 4.2 %copy-start.8 = (bf16[2,4,128,128]{3,2,1,0:T(8,128)(2,1)S(1)}, bf16[2,4,128,128]{3,2,1,0:T(8,128)(2,1)}, u32[]{:S(2)}) copy-start(bf16[2,4,128,128]{3,2,1,0:T(8,128)(2,1)} %param.23) | copy-start | bytes 786436
  17.6 5.1 %copy-start.13 = (f32[2,512]{1,0:T(2,128)S(1)}, f32[2,512]{1,0:T(2,128)}, u32[]{:S(2)}) copy-start(f32[2,512]{1,0:T(2,128)} %param.25) | copy-start | bytes 12292
  20.0 47.1 %collective-permute-start = (bf16[512,2048]{1,0:T(8,128)(2,1)}, bf16[512,2048]{1,0:T(8,128)(2,1)}, u32[]{:S(2)}, u32[]{:S(2)}) collective-permute-start(bf16[512,2048]{1,0:T(8,128)(2,1)} %fusion.2), channel_id=1, source_target_pairs={{0,1},{1,0},{2,3},{3,2},{4,5},{5,4},{6,7},{7,6},{8,9},{9,8},{10,11... | collective-permute-start | bytes 6291464 | tf_op jit(solution)/shard_map/ppermute | solution.py:191
  119.6 14.2 %collective-permute-start.2 = (bf16[512,512]{1,0:T(8,128)(2,1)S(1)}, bf16[512,512]{1,0:T(8,128)(2,1)S(1)}, u32[]{:S(2)}, u32[]{:S(2)}) collective-permute-start(bf16[512,512]{1,0:T(8,128)(2,1)S(1)} %constant_dynamic-slice_fusion), channel_id=1, source_target_pairs={{0,1},{1,0},{2,3},{3,2},{4,5},{5,4},{6,7},{7,6},{8,9},{9,8},{10,11... | collective-permute-start | bytes 1572872 | tf_op jit(solution)/shard_map/ppermute | solution.py:191
  121.1 15.6 %copy-start.6 = (bf16[1024,512]{1,0:T(8,128)(2,1)S(1)}, bf16[1024,512]{1,0:T(8,128)(2,1)}, u32[]{:S(2)}) copy-start(bf16[1024,512]{1,0:T(8,128)(2,1)} %shard_map.145) | copy-start | bytes 3145732
  136.7 3.0 %copy-start.10 = (f32[2048]{0:T(1024)S(1)}, f32[2048]{0:T(1024)}, u32[]{:S(2)}) copy-start(f32[2048]{0:T(1024)} %param.17) | copy-start | bytes 24580
  139.7 1.1 copy-start.11
  140.8 2.0 copy-start.1
  141.4 61.6 %copy-start.3 = (bf16[512,2048]{1,0:T(8,128)(2,1)}, bf16[512,2048]{1,0:T(8,128)(2,1)S(1)}, u32[]{:S(2)}) copy-start(bf16[512,2048]{1,0:T(8,128)(2,1)S(1)} %fusion.6.x_ref) | copy-start | bytes 6291460
  142.8 26.0 %collective-permute-start.3 = (bf16[256,2048]{1,0:T(8,128)(2,1)S(1)}, bf16[256,2048]{1,0:T(8,128)(2,1)S(1)}, u32[]{:S(2)}, u32[]{:S(2)}) collective-permute-start(bf16[256,2048]{1,0:T(8,128)(2,1)S(1)} %get-tuple-element.9), channel_id=1, source_target_pairs={{0,1},{1,0},{2,3},{3,2},{4,5},{5,4},{6,7},{7,6},{8,9},{9,8},{10,11... | collective-permute-start | bytes 3145736 | tf_op jit(solution)/shard_map/ppermute | solution.py:191
  144.2 60.2 %collective-permute-start.5 = (bf16[256,2048]{1,0:T(8,128)(2,1)}, bf16[256,2048]{1,0:T(8,128)(2,1)}, u32[]{:S(2)}, u32[]{:S(2)}) collective-permute-start(bf16[256,2048]{1,0:T(8,128)(2,1)} %get-tuple-element.10), channel_id=1, source_target_pairs={{0,1},{1,0},{2,3},{3,2},{4,5},{5,4},{6,7},{7,6},{8,9},{9,8},{10,11... | collective-permute-start | bytes 3145736 | tf_op jit(solution)/shard_map/ppermute | solution.py:191
  168.8 21.4 %copy-start.5 = (bf16[256,2048]{1,0:T(8,128)(2,1)}, bf16[256,2048]{1,0:T(8,128)(2,1)S(1)}, u32[]{:S(2)}) copy-start(bf16[256,2048]{1,0:T(8,128)(2,1)S(1)} %collective-permute-done.3.x_ref) | copy-start | bytes 3145732
  203.0 32.6 %collective-permute-start.4 = (bf16[256,2048]{1,0:T(8,128)(2,1)}, bf16[256,2048]{1,0:T(8,128)(2,1)S(1)}, u32[]{:S(2)}, u32[]{:S(2)}) collective-permute-start(bf16[256,2048]{1,0:T(8,128)(2,1)} %shard_map.147), channel_id=1, source_target_pairs={{0,1},{1,0},{2,3},{3,2},{4,5},{5,4},{6,7},{7,6},{8,9},{9,8},{10,11... | collective-permute-start | bytes 3145736 | tf_op jit(solution)/shard_map/ppermute | solution.py:191
  217.2 33.7 %collective-permute-start.6 = (bf16[256,2048]{1,0:T(8,128)(2,1)}, bf16[256,2048]{1,0:T(8,128)(2,1)S(1)}, u32[]{:S(2)}, u32[]{:S(2)}) collective-permute-start(bf16[256,2048]{1,0:T(8,128)(2,1)} %shard_map.148), channel_id=1, source_target_pairs={{0,1},{1,0},{2,3},{3,2},{4,5},{5,4},{6,7},{7,6},{8,9},{9,8},{10,11... | collective-permute-start | bytes 3145736 | tf_op jit(solution)/shard_map/ppermute | solution.py:191
  217.8 35.5 %copy-start.12 = (f32[2048]{0:T(1024)S(1)}, f32[2048]{0:T(1024)}, u32[]{:S(2)}) copy-start(f32[2048]{0:T(1024)} %param.19) | copy-start | bytes 24580
  235.5 17.8 %copy-start.2 = (bf16[512,2048]{1,0:T(8,128)(2,1)S(1)}, bf16[512,2048]{1,0:T(8,128)(2,1)}, u32[]{:S(2)}) copy-start(bf16[512,2048]{1,0:T(8,128)(2,1)} %copy-done.1) | copy-start | bytes 6291460
  235.5 17.8 %copy-start.4 = (bf16[512,2048]{1,0:T(8,128)(2,1)S(1)}, bf16[512,2048]{1,0:T(8,128)(2,1)}, u32[]{:S(2)}) copy-start(bf16[512,2048]{1,0:T(8,128)(2,1)} %shard_map.146) | copy-start | bytes 6291460
Sparse Core Ops, SparseCore 0:
  15.3 75.7 all-gather.2
  92.7 97.4 all-gather.4

commit v2 on v1

--- a/solution.py
+++ b/solution.py
@@ -187,6 +187,136 @@
     )(x, weights, weights, weights)
 
 
+def ring_chip(place, chips):
+    half = chips // 2
+    turned = place // half
+    row = place * (1 - turned) + (chips - 1 - place) * turned
+    return row * 2 + turned
+
+
+def ring_kernel(
+    size, shard_ref, x_ref, out_ref, seq_ref, own_sem, send, recv, near_send, near_recv, swap_sem
+):
+    chips = size // 2
+    me = lax.axis_index("fs")
+    core = me % 2
+    turned = (me // 2) % 2
+    row = me // 4
+    place = row * (1 - turned) + (chips - 1 - row) * turned
+    partner = me + 1 - 2 * core
+    after = ring_chip((place + 1) % chips, chips) * 2 + core
+    before = ring_chip((place + chips - 1) % chips, chips) * 2 + core
+    targets = ({"fs": after}, {"fs": before})
+    partner = {"fs": partner}
+    column = lax.axis_index("tp")
+    across = {"tp": 1 - column}
+
+    barrier = pltpu.get_barrier_semaphore()
+    for device in (*targets, partner, across):
+        pl.semaphore_signal(
+            barrier, inc=1, device_id=device, device_id_type=pl.DeviceIdType.MESH
+        )
+    pl.semaphore_wait(barrier, 4)
+
+    depth = shard_ref.shape[0]
+    half = depth // 2
+
+    def remote(src, dst, sent, landed, device):
+        copy = pltpu.make_async_remote_copy(
+            src_ref=src,
+            dst_ref=dst,
+            send_sem=sent,
+            recv_sem=landed,
+            device_id=device,
+            device_id_type=pl.DeviceIdType.MESH,
+        )
+        copy.start()
+        return copy
+
+    def rows_of(origin, side):
+        start = pl.multiple_of(origin * depth + side * half, half)
+        return out_ref.at[pl.ds(start, half), :]
+
+    moving = []
+    for side in range(2):
+        moving.append(
+            remote(
+                shard_ref.at[pl.ds(side * half, half), :],
+                rows_of(me, side),
+                send.at[side, 0],
+                recv.at[side, 0],
+                targets[side],
+            )
+        )
+    waiting = list(moving)
+    count = x_ref.shape[0]
+    own_rows = seq_ref.at[pl.ds(pl.multiple_of(column * count, count), count), :]
+    near = [remote(x_ref, own_rows, swap_sem.at[0], swap_sem.at[1], across)]
+    mine = out_ref.at[pl.ds(pl.multiple_of(me * depth, depth), depth), :]
+    near.append(remote(shard_ref, mine, near_send.at[0, 0], near_recv.at[0, 0], partner))
+    own = pltpu.make_async_copy(shard_ref, mine, own_sem.at[0])
+    own.start()
+    kept = pltpu.make_async_copy(x_ref, own_rows, own_sem.at[1])
+    kept.start()
+    for step in range(chips - 1):
+        for side in range(2):
+            moving[side].wait_recv()
+            back = step + 1 if side == 0 else chips - 1 - step
+            origin = ring_chip((place + chips - back) % chips, chips) * 2 + core
+            piece = rows_of(origin, side)
+            if step < chips - 2:
+                moving[side] = remote(
+                    piece,
+                    piece,
+                    send.at[side, step + 1],
+                    recv.at[side, step + 1],
+                    targets[side],
+                )
+                waiting.append(moving[side])
+            near.append(
+                remote(
+                    piece,
+                    piece,
+                    near_send.at[side, step + 1],
+                    near_recv.at[side, step + 1],
+                    partner,
+                )
+            )
+    for copy in waiting:
+        copy.wait_send()
+    for copy in near:
+        copy.wait()
+    own.wait()
+    kept.wait()
+
+
+def ring_gather(shard, x, size):
+    rows, width = shard.shape
+    chips = size // 2
+    dma = pltpu.SemaphoreType.DMA
+    return pl.pallas_call(
+        functools.partial(ring_kernel, size),
+        out_shape=(
+            jax.ShapeDtypeStruct((rows * size, width), shard.dtype),
+            jax.ShapeDtypeStruct((2 * x.shape[0], x.shape[1]), x.dtype),
+        ),
+        in_specs=[pl.BlockSpec(memory_space=pl.ANY)] * 2,
+        out_specs=(pl.BlockSpec(memory_space=pl.ANY), pl.BlockSpec(memory_space=pl.ANY)),
+        scratch_shapes=[
+            dma((2,)),
+            dma((2, chips)),
+            dma((2, chips)),
+            dma((2, chips)),
+            dma((2, chips)),
+            dma((2,)),
+        ],
+        compiler_params=pltpu.CompilerParams(collective_id=0, has_side_effects=True),
+        cost_estimate=pl.CostEstimate(
+            flops=1 << 32, bytes_accessed=2 * rows * size * width, transcendentals=0
+        ),
+    )(shard, x)
+
+
 def swap(values):
     return lax.ppermute(values, "tp", [(0, 1), (1, 0)])
 
@@ -221,19 +351,17 @@
     parts = [w_branch, w_gelu, out_weight_t]
     if pair:
         parts.append(swap(out_weight_t))
-    mix_all = lax.all_gather(jnp.concatenate(parts, axis=1), "fs", axis=0, tiled=True)
-    ffn_all = lax.all_gather(
-        jnp.concatenate([w_gate, w_up, down_weight_t], axis=1), "fs", axis=0, tiled=True
-    )
+    mix_shard = jnp.concatenate(parts, axis=1)
+    ffn_shard = jnp.concatenate([w_gate, w_up, down_weight_t], axis=1)
     stream = tokens.astype(jnp.float32)
     normed_in = normed(stream, pre_mix_gain).astype(jnp.bfloat16)
     if pair:
-        other = swap(normed_in)
-        first = jnp.where(place == 0, normed_in, other)
-        second = jnp.where(place == 0, other, normed_in)
-        sequence = jnp.concatenate([first, second], axis=0)
+        mix_all, sequence = ring_gather(mix_shard, normed_in, lax.axis_size("fs"))
+        ffn_shard, mix_all = lax.optimization_barrier((ffn_shard, mix_all))
     else:
+        mix_all = lax.all_gather(mix_shard, "fs", axis=0, tiled=True)
         sequence = lax.all_gather(normed_in, "tp", axis=0, tiled=True)
+    ffn_all = lax.all_gather(ffn_shard, "fs", axis=0, tiled=True)
     hidden = mixer(sequence, mix_all, conv_weight, w_rec, w_inp, decay)
     out_own = mix_all[:, 2 * channels : 3 * channels]
     if pair:

time: 264 us -> 272 us (1.030)
  Pallas kernels: 70.7 us -> 153 us
  waiting for transfers between devices: 139 us -> 72.4 us
  other arithmetic: 21 us -> 15.6 us
    pallas_call x0 -> x1, Pallas kernels: none -> 82.7 us  [ring_gather(): pl.pallas_call(functools.partial(ring_kernel, size), out_shape=(jax.Shape...]
    ppermute x7 -> x6, waiting for transfers between devices: 99.6 us -> 48.8 us  [swap(): return lax.ppermute(values, 'tp', [(0, 1), (1, 0)])]
    all_gather x2 -> x1, waiting for transfers between devices: 39.5 us -> 23.6 us  [per_device(): ffn_all = lax.all_gather(ffn_shard, 'fs', axis=0, tiled=True)]
    concatenate x3 -> x2, other arithmetic: 6.94 us -> 3.24 us  [the longest x1 2.37 us: per_device(): ffn_shard = jnp.concatenate([w_gate, w_up, down_weight_t], axis=1)]
    select_n x1 -> x0, other arithmetic: 3.22 us -> none  [per_device(): first = jnp.where(place == 0, normed_in, other)]
    ppermute x7 -> x6, starting transfers between devices: 10.3 us -> 7.85 us  [swap(): return lax.ppermute(values, 'tp', [(0, 1), (1, 0)])]
  transfers between devices with their start and end apart: 9 -> 7, of which waited for: 7 -> 4; matrix products, arithmetic and copies ran while one was open for 8% -> 7% of each run, Pallas kernels for 27% -> 26%
where the time goes in v2:
time: 272 us
  Pallas kernels  153 us (56%)
  waiting for transfers between devices  72.4 us (27%)
  other arithmetic  15.6 us (6%)
  between operations  13.6 us (5%)
  starting transfers between devices  7.89 us (3%)
  matrix products  6.06 us (2%)
  local copies, waits for them, and re-layouts  2.77 us (1%)
    pallas_call x1, Pallas kernels, ring_gather(): pl.pallas_call(functools.partial(ring_kernel, size), out_shape=(jax.Shape...  82.7 us
    ppermute x6, waiting for transfers between devices, swap(): return lax.ppermute(values, 'tp', [(0, 1), (1, 0)])  48.8 us
    pallas_call x3, Pallas kernels, ffn(): pl.pallas_call(ffn_kernel, grid=(count,), out_shape=jax.ShapeDtypeStruct(...  43.3 us
    pallas_call x1, Pallas kernels, mixer(): pl.pallas_call(mixer_kernel, grid=(count,), out_shape=jax.ShapeDtypeStruc...  27.4 us
    all_gather x1, waiting for transfers between devices, per_device(): ffn_all = lax.all_gather(ffn_shard, 'fs', axis=0, tiled=True)  23.6 us
    ppermute x6, starting transfers between devices, swap(): return lax.ppermute(values, 'tp', [(0, 1), (1, 0)])  7.85 us
    dot_general x2, matrix products, matmul_t(): lax.dot_general(rows, weight_t, (((1,), (1,)), ((), ())), preferred_eleme...  6.06 us
    reduce_sum x3, other arithmetic, normed(): factor = lax.rsqrt(jnp.mean(values * values, axis=-1, keepdims=True) + EPS)  5.49 us
  transfers between devices with their start and end apart: 7, of which 4 were waited for; matrix products, arithmetic and copies ran while one was open for 7% of the time, Pallas kernels for 26%

profile of v2, /device:TPU:0, one launch (start us, length us, event | category | flops | bytes accessed | tf_op | source)
XLA Modules:
  0.0 271.8 jit_solution(10160704958579128782)
XLA Ops:
  6.5 0.0 copy-start.8
  6.5 0.0 copy-start
  6.5 0.0 copy-start.11
  6.5 0.0 copy-start.10
  6.5 0.0 copy-start.9
  6.5 0.0 all-gather.2.cloned.1.call-start
  6.6 3.0 %collective-permute-start = (bf16[128,512]{1,0:T(8,128)(2,1)}, bf16[128,512]{1,0:T(8,128)(2,1)S(1)}, u32[]{:S(2)}, u32[]{:S(2)}) collective-permute-start(bf16[128,512]{1,0:T(8,128)(2,1)} %param.26), channel_id=1, source_target_pairs={{0,1},{1,0},{2,3},{3,2},{4,5},{5,4},{6,7},{7,6},{8,9},{9,8},{10,11... | collective-permute-start | bytes 393224 | tf_op jit(solution)/shard_map/ppermute | solution.py:321
  9.6 2.1 fusion
  11.7 2.4 pad_maximum_fusion.1
  14.1 0.0 copy-done
  14.1 0.0 copy-done.11
  14.1 1.9 fusion.2.x_ref
  15.9 0.0 collective-permute-done
  16.0 0.0 copy-done.8
  16.0 0.0 copy-done.10
  16.0 0.0 copy-done.9
  16.0 0.9 pad_maximum_fusion.2.shard_ref
  16.8 0.0 copy-start.6
  16.8 0.0 copy-start.7
  16.8 0.0 copy-start.15
  16.8 82.7 %shard_map.145 = (bf16[2048,2048]{1,0:T(8,128)(2,1)}, bf16[1024,2048]{1,0:T(8,128)(2,1)}) custom-call(bf16[128,2048]{1,0:T(8,128)(2,1)} %pad_maximum_fusion.2.shard_ref, bf16[512,2048]{1,0:T(8,128)(2,1)} %fusion.2.x_ref), custom_call_target="tpu_custom_call" | custom-call | flops 4294967296 | bytes 8388608 | tf_op jit(solution)/shard_map/pallas_call | solution.py:297
  99.5 0.0 all-gather.2.cloned.1.call-update
  99.6 0.0 copy-done.6
  99.6 0.0 copy-done.7
  99.6 0.9 pad_maximum_fusion.3.gates_ref
  100.5 0.0 copy-done.15
  100.5 0.6 fusion.12.coef_ref
  101.1 27.4 %shard_map.146 = bf16[1024,512]{1,0:T(8,128)(2,1)} custom-call(bf16[1024,2048]{1,0:T(8,128)(2,1)} %get-tuple-element.9.x_ref, bf16[2048,2048]{1,0:T(8,128)(2,1)} %get-tuple-element.11.wb_ref.wg_ref, bf16[2048,2048]{1,0:T(8,128)(2,1)} %get-tuple-element.11.wb_ref.wg_ref, bf16[4,512]{1,0:T(4,128)(2,1)} %conv_ref.1, ...), custom_call_target="tpu_custom_call" | custom-call | flops 12884901888 | bytes 9437184 | tf_op jit(solution)/shard_map/pallas_call | solution.py:118
  128.6 1.1 constant_dynamic-slice_fusion
  129.7 0.8 collective-permute-start.1
  130.4 3.0 %fusion.9 = f32[512,2048]{1,0:T(8,128)S(1)} fusion(bf16[2048,2048]{1,0:T(8,128)(2,1)} %get-tuple-element.11.wb_ref.wg_ref, bf16[1024,512]{1,0:T(8,128)(2,1)} %shard_map.146, s32[]{:T(128)S(6)} %select_n.11), kind=kOutput, calls=%fused_computation.20 | convolution fusion | flops 1073741824 | bytes 6815748 | tf_op jit(solution)/shard_map/dot_general | solution.py:325
  133.5 0.0 copy-start.12
  133.5 9.4 %collective-permute-done.1 = bf16[512,512]{1,0:T(8,128)(2,1)S(1)} collective-permute-done((bf16[512,512]{1,0:T(8,128)(2,1)S(1)}, bf16[512,512]{1,0:T(8,128)(2,1)S(1)}, u32[]{:S(2)}, u32[]{:S(2)}) %collective-permute-start.1) | collective-permute-done | bytes 524320 | tf_op jit(solution)/shard_map/ppermute | solution.py:321
  142.9 3.0 %multiply_reduce_fusion.1 = (f32[512]{0:T(512)S(1)}, f32[512,2048]{1,0:T(8,128)S(1)}) fusion(f32[512,2048]{1,0:T(8,128)S(1)} %fusion.9, bf16[512,512]{1,0:T(8,128)(2,1)S(1)} %collective-permute-done.1, bf16[2048,2048]{1,0:T(8,128)(2,1)} %get-tuple-element.11.wb_ref.wg_ref), kind=kOutput, calls=%fused_computation.16 | convolution fusion | flops 1076887040 | bytes 11012096 | tf_op jit(solution)/shard_map/dot_general | solution.py:325
  145.9 0.0 copy-done.12
  145.9 0.0 copy-start.13
  145.9 1.1 fusion.4
  147.0 0.0 copy-start.1
  147.0 0.0 copy-done.13
  147.0 0.6 fusion.6.x_ref
  147.6 0.0 copy-start.3
  147.6 1.6 fusion.15
  149.2 0.0 copy-done.1
  149.2 0.7 collective-permute-start.2
  149.9 1.3 collective-permute-start.4
  151.2 24.0 %collective-permute-done.2.x_ref = bf16[256,2048]{1,0:T(8,128)(2,1)S(1)} collective-permute-done((bf16[256,2048]{1,0:T(8,128)(2,1)S(1)}, bf16[256,2048]{1,0:T(8,128)(2,1)S(1)}, u32[]{:S(2)}, u32[]{:S(2)}) %collective-permute-start.2) | collective-permute-done | bytes 1048608 | tf_op jit(solution)/shard_map/ppermute | solution.py:321
  175.2 0.0 copy-start.5
  175.2 23.6 %all-gather.2.cloned.1.call-done.gate_ref.up_ref.down_ref = bf16[2048,4608]{1,0:T(8,128)(2,1)} async-done(((bf16[128,4608]{1,0:T(8,128)(2,1)}), bf16[2048,4608]{1,0:T(8,128)(2,1)}) %all-gather.2.cloned.1.call-update) | async-done | bytes 18874384 | tf_op jit(solution)/shard_map/all_gather | solution.py:364
  198.8 0.0 copy-done.5
  198.8 12.7 %shard_map.148 = bf16[256,2048]{1,0:T(8,128)(2,1)} custom-call(bf16[256,2048]{1,0:T(8,128)(2,1)} %copy-done.5, bf16[2048,4608]{1,0:T(8,128)(2,1)} %all-gather.2.cloned.1.call-done.gate_ref.up_ref.down_ref, bf16[2048,4608]{1,0:T(8,128)(2,1)} %all-gather.2.cloned.1.call-done.gate_ref.up_ref.down_ref, ...), custom_call_target="tpu_custom_call" | custom-call | flops 4831838208 | bytes 20971520 | tf_op jit(solution)/shard_map/pallas_call | solution.py:169
  211.6 0.0 copy-done.3
  211.6 1.5 collective-permute-start.3
  213.0 0.0 collective-permute-done.4.x_ref
  213.0 12.8 %shard_map.149 = bf16[256,2048]{1,0:T(8,128)(2,1)} custom-call(bf16[256,2048]{1,0:T(8,128)(2,1)} %collective-permute-done.4.x_ref, bf16[2048,4608]{1,0:T(8,128)(2,1)} %all-gather.2.cloned.1.call-done.gate_ref.up_ref.down_ref, bf16[2048,4608]{1,0:T(8,128)(2,1)} %all-gather.2.cloned.1.call-done.gate_ref.up_ref.down_ref, ...), custom_call_target="tpu_custom_call" | custom-call | flops 4831838208 | bytes 20971520 | tf_op jit(solution)/shard_map/pallas_call | solution.py:169
  225.8 0.6 collective-permute-start.5
  226.4 0.0 copy-start.14
  226.4 17.8 %shard_map.147 = bf16[512,2048]{1,0:T(8,128)(2,1)} custom-call(bf16[512,2048]{1,0:T(8,128)(2,1)} %copy-done.3, bf16[2048,4608]{1,0:T(8,128)(2,1)} %all-gather.2.cloned.1.call-done.gate_ref.up_ref.down_ref, bf16[2048,4608]{1,0:T(8,128)(2,1)} %all-gather.2.cloned.1.call-done.gate_ref.up_ref.down_ref, ...), custom_call_target="tpu_custom_call" | custom-call | flops 9663676416 | bytes 23068672 | tf_op jit(solution)/shard_map/pallas_call | solution.py:169
  244.1 0.0 collective-permute-done.3
  244.1 15.4 %collective-permute-done.5 = bf16[256,2048]{1,0:T(8,128)(2,1)S(1)} collective-permute-done((bf16[256,2048]{1,0:T(8,128)(2,1)}, bf16[256,2048]{1,0:T(8,128)(2,1)S(1)}, u32[]{:S(2)}, u32[]{:S(2)}) %collective-permute-start.5) | collective-permute-done | bytes 1048608 | tf_op jit(solution)/shard_map/ppermute | solution.py:321
  259.6 2.3 multiply_reduce_fusion
  261.9 0.0 copy-done.14
  261.9 0.0 copy-done.2
  261.9 0.0 copy-done.4
  261.9 3.0 %fusion.7 = bf16[512,2048]{1,0:T(8,128)(2,1)} fusion(bf16[512,2048]{1,0:T(8,128)(2,1)S(1)} %copy-done.2, bf16[512,2048]{1,0:T(8,128)(2,1)S(1)} %copy-done.4, f32[2048]{0:T(1024)S(1)} %copy-done.14, f32[512]{0:T(512)S(1)} %add_rsqrt_fusion, bf16[256,2048]{1,0:T(8,128)(2,1)S(1)} %collective-permute-done.5, bf16[256,2048]{1,0:T(8,128)(2,1)S(1)} %collective-permute-done.3), kind=kLoop, calls=%fused_computation.13 | loop fusion | flops 11534336 | bytes 8398848 | tf_op jit(solution)/shard_map/convert_element_type | solution.py:392
  (7 shorter events, 0.1 us)
Async XLA Ops:
  6.5 9.4 %copy-start.8 = (bf16[128,512]{1,0:T(8,128)(2,1)S(1)}, bf16[128,512]{1,0:T(8,128)(2,1)}, u32[]{:S(2)}) copy-start(bf16[128,512]{1,0:T(8,128)(2,1)} %param.26) | copy-start | bytes 393220
  6.5 7.5 %copy-start = (bf16[512,2048]{1,0:T(8,128)(2,1)S(1)}, bf16[512,2048]{1,0:T(8,128)(2,1)}, u32[]{:S(2)}) copy-start(bf16[512,2048]{1,0:T(8,128)(2,1)} %param.15) | copy-start | bytes 6291460
  6.5 7.5 %copy-start.11 = (f32[2048]{0:T(1024)S(1)}, f32[2048]{0:T(1024)}, u32[]{:S(2)}) copy-start(f32[2048]{0:T(1024)} %param.16) | copy-start | bytes 24580
  6.5 9.4 %copy-start.10 = (bf16[128,512]{1,0:T(8,128)(2,1)S(1)}, bf16[128,512]{1,0:T(8,128)(2,1)}, u32[]{:S(2)}) copy-start(bf16[128,512]{1,0:T(8,128)(2,1)} %param.20) | copy-start | bytes 393220
  6.5 9.4 %copy-start.9 = (bf16[128,512]{1,0:T(8,128)(2,1)S(1)}, bf16[128,512]{1,0:T(8,128)(2,1)}, u32[]{:S(2)}) copy-start(bf16[128,512]{1,0:T(8,128)(2,1)} %param.21) | copy-start | bytes 393220
  6.5 192.3 %all-gather.2.cloned.1.call-start = ((), (), s32[]{:S(2)}) async-start(), calls=%async_computation | async-start | bytes 20054016 | tf_op jit(solution)/shard_map/all_gather | solution.py:364
  6.6 9.4 %collective-permute-start = (bf16[128,512]{1,0:T(8,128)(2,1)}, bf16[128,512]{1,0:T(8,128)(2,1)S(1)}, u32[]{:S(2)}, u32[]{:S(2)}) collective-permute-start(bf16[128,512]{1,0:T(8,128)(2,1)} %param.26), channel_id=1, source_target_pairs={{0,1},{1,0},{2,3},{3,2},{4,5},{5,4},{6,7},{7,6},{8,9},{9,8},{10,11... | collective-permute-start | bytes 393224 | tf_op jit(solution)/shard_map/ppermute | solution.py:321
  16.8 82.7 %copy-start.6 = (bf16[2,4,128,128]{3,2,1,0:T(8,128)(2,1)S(1)}, bf16[2,4,128,128]{3,2,1,0:T(8,128)(2,1)}, u32[]{:S(2)}) copy-start(bf16[2,4,128,128]{3,2,1,0:T(8,128)(2,1)} %param.24) | copy-start | bytes 786436
  16.8 82.7 %copy-start.7 = (bf16[2,4,128,128]{3,2,1,0:T(8,128)(2,1)S(1)}, bf16[2,4,128,128]{3,2,1,0:T(8,128)(2,1)}, u32[]{:S(2)}) copy-start(bf16[2,4,128,128]{3,2,1,0:T(8,128)(2,1)} %param.23) | copy-start | bytes 786436
  16.8 83.7 %copy-start.15 = (f32[2,512]{1,0:T(2,128)S(1)}, f32[2,512]{1,0:T(2,128)}, u32[]{:S(2)}) copy-start(f32[2,512]{1,0:T(2,128)} %param.25) | copy-start | bytes 12292
  129.7 13.2 %collective-permute-start.1 = (bf16[512,512]{1,0:T(8,128)(2,1)S(1)}, bf16[512,512]{1,0:T(8,128)(2,1)S(1)}, u32[]{:S(2)}, u32[]{:S(2)}) collective-permute-start(bf16[512,512]{1,0:T(8,128)(2,1)S(1)} %constant_dynamic-slice_fusion), channel_id=1, source_target_pairs={{0,1},{1,0},{2,3},{3,2},{4,5},{5,4},{6,7},{7,6},{8,9},{9,8},{10,11... | collective-permute-start | bytes 1572872 | tf_op jit(solution)/shard_map/ppermute | solution.py:321
  133.5 12.4 %copy-start.12 = (f32[2048]{0:T(1024)S(1)}, f32[2048]{0:T(1024)}, u32[]{:S(2)}) copy-start(f32[2048]{0:T(1024)} %param.17) | copy-start | bytes 24580
  145.9 1.1 copy-start.13
  147.0 2.2 copy-start.1
  147.6 64.0 %copy-start.3 = (bf16[512,2048]{1,0:T(8,128)(2,1)}, bf16[512,2048]{1,0:T(8,128)(2,1)S(1)}, u32[]{:S(2)}) copy-start(bf16[512,2048]{1,0:T(8,128)(2,1)S(1)} %fusion.6.x_ref) | copy-start | bytes 6291460
  149.2 26.0 %collective-permute-start.2 = (bf16[256,2048]{1,0:T(8,128)(2,1)S(1)}, bf16[256,2048]{1,0:T(8,128)(2,1)S(1)}, u32[]{:S(2)}, u32[]{:S(2)}) collective-permute-start(bf16[256,2048]{1,0:T(8,128)(2,1)S(1)} %get-tuple-element.15), channel_id=1, source_target_pairs={{0,1},{1,0},{2,3},{3,2},{4,5},{5,4},{6,7},{7,6},{8,9},{9,8},{10,11... | collective-permute-start | bytes 3145736 | tf_op jit(solution)/shard_map/ppermute | solution.py:321
  149.9 63.1 %collective-permute-start.4 = (bf16[256,2048]{1,0:T(8,128)(2,1)}, bf16[256,2048]{1,0:T(8,128)(2,1)}, u32[]{:S(2)}, u32[]{:S(2)}) collective-permute-start(bf16[256,2048]{1,0:T(8,128)(2,1)} %get-tuple-element.16), channel_id=1, source_target_pairs={{0,1},{1,0},{2,3},{3,2},{4,5},{5,4},{6,7},{7,6},{8,9},{9,8},{10,11... | collective-permute-start | bytes 3145736 | tf_op jit(solution)/shard_map/ppermute | solution.py:321
  175.2 23.6 %copy-start.5 = (bf16[256,2048]{1,0:T(8,128)(2,1)}, bf16[256,2048]{1,0:T(8,128)(2,1)S(1)}, u32[]{:S(2)}) copy-start(bf16[256,2048]{1,0:T(8,128)(2,1)S(1)} %collective-permute-done.2.x_ref) | copy-start | bytes 3145732
  211.6 32.6 %collective-permute-start.3 = (bf16[256,2048]{1,0:T(8,128)(2,1)}, bf16[256,2048]{1,0:T(8,128)(2,1)S(1)}, u32[]{:S(2)}, u32[]{:S(2)}) collective-permute-start(bf16[256,2048]{1,0:T(8,128)(2,1)} %shard_map.148), channel_id=1, source_target_pairs={{0,1},{1,0},{2,3},{3,2},{4,5},{5,4},{6,7},{7,6},{8,9},{9,8},{10,11... | collective-permute-start | bytes 3145736 | tf_op jit(solution)/shard_map/ppermute | solution.py:321
  225.8 33.7 %collective-permute-start.5 = (bf16[256,2048]{1,0:T(8,128)(2,1)}, bf16[256,2048]{1,0:T(8,128)(2,1)S(1)}, u32[]{:S(2)}, u32[]{:S(2)}) collective-permute-start(bf16[256,2048]{1,0:T(8,128)(2,1)} %shard_map.149), channel_id=1, source_target_pairs={{0,1},{1,0},{2,3},{3,2},{4,5},{5,4},{6,7},{7,6},{8,9},{9,8},{10,11... | collective-permute-start | bytes 3145736 | tf_op jit(solution)/shard_map/ppermute | solution.py:321
  226.4 35.5 %copy-start.14 = (f32[2048]{0:T(1024)S(1)}, f32[2048]{0:T(1024)}, u32[]{:S(2)}) copy-start(f32[2048]{0:T(1024)} %param.19) | copy-start | bytes 24580
  244.1 17.8 %copy-start.2 = (bf16[512,2048]{1,0:T(8,128)(2,1)S(1)}, bf16[512,2048]{1,0:T(8,128)(2,1)}, u32[]{:S(2)}) copy-start(bf16[512,2048]{1,0:T(8,128)(2,1)} %copy-done.1) | copy-start | bytes 6291460
  244.1 17.8 %copy-start.4 = (bf16[512,2048]{1,0:T(8,128)(2,1)S(1)}, bf16[512,2048]{1,0:T(8,128)(2,1)}, u32[]{:S(2)}) copy-start(bf16[512,2048]{1,0:T(8,128)(2,1)} %shard_map.147) | copy-start | bytes 6291460
Sparse Core Ops, SparseCore 0:
  99.7 99.0 all-gather.1

commit v3 on v2

--- a/solution.py
+++ b/solution.py
@@ -9,6 +9,7 @@
 
 EPS = 1e-06
 SEGMENTS = 8
+PIECES = 4
 VMEM_BYTES = 60 * 1024 * 1024
 
 
@@ -25,21 +26,28 @@
 
 
 def mixer_kernel(
-    x_ref, wb_ref, wg_ref, conv_ref, gates_ref, coef_ref, out_ref, pad, gel, a0, u0, a1, u1
+    paired, x_ref, y_ref, wb_ref, wg_ref, conv_ref, gates_ref, coef_ref, out_ref, pad, gel, a0, u0, a1, u1
 ):
     length, width = out_ref.shape
     group = gates_ref.shape[1]
     rows = 256
     pad[0:8, :] = jnp.zeros((8, width), jnp.float32)
     pad[8 + length : 16 + length, :] = jnp.zeros((8, width), jnp.float32)
-    for start in range(0, length, rows):
-        piece = x_ref[start : start + rows, :]
-        branch = jnp.dot(piece, wb_ref[...], preferred_element_type=jnp.float32)
-        pad[8 + start : 8 + start + rows, :] = branch.astype(jnp.bfloat16).astype(jnp.float32)
-        gelu_in = jnp.dot(piece, wg_ref[...], preferred_element_type=jnp.float32)
-        gel[start : start + rows, :] = jax.nn.gelu(
-            gelu_in.astype(jnp.bfloat16).astype(jnp.float32)
-        )
+    if paired:
+        own_start = lax.axis_index("tp") * x_ref.shape[0]
+        sources = ((x_ref, own_start), (y_ref, x_ref.shape[0] - own_start))
+    else:
+        sources = ((x_ref, 0),)
+    for source, base in sources:
+        for start in range(0, source.shape[0], rows):
+            piece = source[start : start + rows, :]
+            branch = jnp.dot(piece, wb_ref[...], preferred_element_type=jnp.float32)
+            gelu_in = jnp.dot(piece, wg_ref[...], preferred_element_type=jnp.float32)
+            at = pl.multiple_of(base + start, rows)
+            pad[pl.ds(8 + at, rows), :] = branch.astype(jnp.bfloat16).astype(jnp.float32)
+            gel[pl.ds(at, rows), :] = jax.nn.gelu(
+                gelu_in.astype(jnp.bfloat16).astype(jnp.float32)
+            )
 
     for part in range(width // group):
         cols = slice(part * group, (part + 1) * group)
@@ -106,8 +114,10 @@
             out_ref[span, lanes] = (gel[span, lanes] * (forward + backward)).astype(jnp.bfloat16)
 
 
-def mixer(x, weights, conv_weight, w_rec, w_inp, decay):
+def mixer(paired, x, y, weights, conv_weight, w_rec, w_inp, decay):
     length, model = x.shape
+    x_spec = pl.BlockSpec((length, model), lambda j: (0, 0))
+    length = 2 * length if paired else length
     channels = conv_weight.shape[1]
     group = w_rec.shape[2]
     width = min(256, channels)
@@ -116,11 +126,12 @@
     coef = -8.0 * jax.nn.softplus(-decay)
     f32 = functools.partial(pltpu.VMEM, dtype=jnp.float32)
     return pl.pallas_call(
-        mixer_kernel,
+        functools.partial(mixer_kernel, paired),
         grid=(count,),
         out_shape=jax.ShapeDtypeStruct((length, channels), jnp.bfloat16),
         in_specs=[
-            pl.BlockSpec((length, model), lambda j: (0, 0)),
+            x_spec,
+            x_spec if paired else pl.BlockSpec((8, model), lambda j: (0, 0)),
             pl.BlockSpec((model, width), lambda j: (0, j)),
             pl.BlockSpec((model, width), lambda j: (0, count + j)),
             pl.BlockSpec((4, width), lambda j: (0, j)),
@@ -136,7 +147,7 @@
             bytes_accessed=2 * (length * model + 2 * model * channels + length * channels),
             transcendentals=12 * length * channels,
         ),
-    )(x, weights, weights, conv_weight, gates, coef)
+    )(x, y, weights, weights, conv_weight, gates, coef)
 
 
 def ffn_kernel(x_ref, gate_ref, up_ref, down_ref, out_ref, total):
@@ -195,7 +206,7 @@
 
 
 def ring_kernel(
-    size, shard_ref, x_ref, out_ref, seq_ref, own_sem, send, recv, near_send, near_recv, swap_sem
+    size, shard_ref, x_ref, out_ref, other_ref, own_sem, send, recv, near_send, near_recv, swap_sem
 ):
     chips = size // 2
     me = lax.axis_index("fs")
@@ -219,7 +230,7 @@
     pl.semaphore_wait(barrier, 4)
 
     depth = shard_ref.shape[0]
-    half = depth // 2
+    piece_rows = depth // (2 * PIECES)
 
     def remote(src, dst, sent, landed, device):
         copy = pltpu.make_async_remote_copy(
@@ -233,52 +244,48 @@
         copy.start()
         return copy
 
-    def rows_of(origin, side):
-        start = pl.multiple_of(origin * depth + side * half, half)
-        return out_ref.at[pl.ds(start, half), :]
+    def rows_of(origin, at):
+        start = pl.multiple_of(origin * depth + at * piece_rows, piece_rows)
+        return out_ref.at[pl.ds(start, piece_rows), :]
 
     moving = []
-    for side in range(2):
+    for at in range(2 * PIECES):
         moving.append(
             remote(
-                shard_ref.at[pl.ds(side * half, half), :],
-                rows_of(me, side),
-                send.at[side, 0],
-                recv.at[side, 0],
-                targets[side],
+                shard_ref.at[pl.ds(at * piece_rows, piece_rows), :],
+                rows_of(me, at),
+                send.at[at, 0],
+                recv.at[at, 0],
+                targets[at % 2],
             )
         )
     waiting = list(moving)
-    count = x_ref.shape[0]
-    own_rows = seq_ref.at[pl.ds(pl.multiple_of(column * count, count), count), :]
-    near = [remote(x_ref, own_rows, swap_sem.at[0], swap_sem.at[1], across)]
+    near = [remote(x_ref, other_ref, swap_sem.at[0], swap_sem.at[1], across)]
     mine = out_ref.at[pl.ds(pl.multiple_of(me * depth, depth), depth), :]
     near.append(remote(shard_ref, mine, near_send.at[0, 0], near_recv.at[0, 0], partner))
-    own = pltpu.make_async_copy(shard_ref, mine, own_sem.at[0])
+    own = pltpu.make_async_copy(shard_ref, mine, own_sem)
     own.start()
-    kept = pltpu.make_async_copy(x_ref, own_rows, own_sem.at[1])
-    kept.start()
     for step in range(chips - 1):
-        for side in range(2):
-            moving[side].wait_recv()
-            back = step + 1 if side == 0 else chips - 1 - step
+        for at in range(2 * PIECES):
+            moving[at].wait_recv()
+            back = step + 1 if at % 2 == 0 else chips - 1 - step
             origin = ring_chip((place + chips - back) % chips, chips) * 2 + core
-            piece = rows_of(origin, side)
+            piece = rows_of(origin, at)
             if step < chips - 2:
-                moving[side] = remote(
+                moving[at] = remote(
                     piece,
                     piece,
-                    send.at[side, step + 1],
-                    recv.at[side, step + 1],
-                    targets[side],
+                    send.at[at, step + 1],
+                    recv.at[at, step + 1],
+                    targets[at % 2],
                 )
-                waiting.append(moving[side])
+                waiting.append(moving[at])
             near.append(
                 remote(
                     piece,
                     piece,
-                    near_send.at[side, step + 1],
-                    near_recv.at[side, step + 1],
+                    near_send.at[at, step + 1],
+                    near_recv.at[at, step + 1],
                     partner,
                 )
             )
@@ -287,7 +294,6 @@
     for copy in near:
         copy.wait()
     own.wait()
-    kept.wait()
 
 
 def ring_gather(shard, x, size):
@@ -298,16 +304,19 @@
         functools.partial(ring_kernel, size),
         out_shape=(
             jax.ShapeDtypeStruct((rows * size, width), shard.dtype),
-            jax.ShapeDtypeStruct((2 * x.shape[0], x.shape[1]), x.dtype),
+            jax.ShapeDtypeStruct(x.shape, x.dtype),
         ),
-        in_specs=[pl.BlockSpec(memory_space=pl.ANY)] * 2,
+        in_specs=[
+            pl.BlockSpec(memory_space=pltpu.VMEM),
+            pl.BlockSpec(memory_space=pl.ANY),
+        ],
         out_specs=(pl.BlockSpec(memory_space=pl.ANY), pl.BlockSpec(memory_space=pl.ANY)),
         scratch_shapes=[
-            dma((2,)),
-            dma((2, chips)),
-            dma((2, chips)),
-            dma((2, chips)),
-            dma((2, chips)),
+            dma,
+            dma((2 * PIECES, chips)),
+            dma((2 * PIECES, chips)),
+            dma((2 * PIECES, chips)),
+            dma((2 * PIECES, chips)),
             dma((2,)),
         ],
         compiler_params=pltpu.CompilerParams(collective_id=0, has_side_effects=True),
@@ -348,27 +357,39 @@
     own_rows = tokens.shape[0]
     channels = conv_weight.shape[1]
     place = lax.axis_index("tp")
-    parts = [w_branch, w_gelu, out_weight_t]
-    if pair:
-        parts.append(swap(out_weight_t))
-    mix_shard = jnp.concatenate(parts, axis=1)
+    mix_shard = jnp.concatenate([w_branch, w_gelu, out_weight_t], axis=1)
     ffn_shard = jnp.concatenate([w_gate, w_up, down_weight_t], axis=1)
     stream = tokens.astype(jnp.float32)
     normed_in = normed(stream, pre_mix_gain).astype(jnp.bfloat16)
     if pair:
-        mix_all, sequence = ring_gather(mix_shard, normed_in, lax.axis_size("fs"))
-        ffn_shard, mix_all = lax.optimization_barrier((ffn_shard, mix_all))
+        fs_size = lax.axis_size("fs")
+        mix_all, other = ring_gather(mix_shard, normed_in, fs_size)
+        ffn_shard, mix_all, other = lax.optimization_barrier((ffn_shard, mix_all, other))
+        sequence = (normed_in, other)
     else:
         mix_all = lax.all_gather(mix_shard, "fs", axis=0, tiled=True)
-        sequence = lax.all_gather(normed_in, "tp", axis=0, tiled=True)
+        whole = lax.all_gather(normed_in, "tp", axis=0, tiled=True)
+        sequence = (whole, whole)
     ffn_all = lax.all_gather(ffn_shard, "fs", axis=0, tiled=True)
-    hidden = mixer(sequence, mix_all, conv_weight, w_rec, w_inp, decay)
-    out_own = mix_all[:, 2 * channels : 3 * channels]
+    out_own = mix_all[:, 2 * channels :]
     if pair:
+        core = lax.axis_index("fs") % 2
+        span = out_own.shape[0] // 2
+        partners = [(i, i + 1 - 2 * (i % 2)) for i in range(fs_size)]
+        crossed = swap(lax.dynamic_slice_in_dim(out_own, core * span, span, 0))
+    hidden = mixer(pair, *sequence, mix_all, conv_weight, w_rec, w_inp, decay)
+    if pair:
+        crossed, hidden = lax.optimization_barrier((crossed, hidden))
+        shared = lax.ppermute(crossed, "fs", partners)
+        out_other = (
+            jnp.where(core == 0, crossed, shared),
+            jnp.where(core == 0, shared, crossed),
+        )
         away = lax.dynamic_slice_in_dim(hidden, (1 - place) * own_rows, own_rows, 0)
         kept = lax.dynamic_slice_in_dim(hidden, place * own_rows, own_rows, 0)
         came = swap(away)
-        mixer_sum = matmul_t(kept, out_own) + matmul_t(came, mix_all[:, 3 * channels :])
+        far = jnp.concatenate(out_other, axis=0)
+        mixer_sum = matmul_t(kept, out_own) + matmul_t(came, far)
     else:
         own_hidden = lax.all_to_all(hidden, "tp", split_axis=0, concat_axis=1, tiled=True)
         out_whole = lax.all_gather(out_own, "tp", axis=1, tiled=True)
@@ -379,7 +400,6 @@
     if pair:
         pieces = 2
         size = own_rows // pieces
-        sums = []
         away_rows = [swap(normed_mid[i * size : (i + 1) * size]) for i in range(pieces)]
         back = [swap(ffn(rows, ffn_all)) for rows in away_rows]
         own_part = ffn(normed_mid, ffn_all).astype(jnp.float32)

time: 272 us -> 242 us (0.89)
  Pallas kernels: 153 us -> 125 us
  waiting for transfers between devices: 72.4 us -> 67.7 us
  local copies, waits for them, and re-layouts: 2.77 us -> 6.49 us
    pallas_call x1, Pallas kernels: 82.7 us -> 53.8 us  [ring_gather(): pl.pallas_call(functools.partial(ring_kernel, size), out_shape=(jax.Shape...]
    all_gather x1, waiting for transfers between devices: 23.6 us -> 15.3 us  [per_device(): ffn_all = lax.all_gather(ffn_shard, 'fs', axis=0, tiled=True)]
    ppermute x6, waiting for transfers between devices: 48.8 us -> 51.9 us  [swap(): return lax.ppermute(values, 'tp', [(0, 1), (1, 0)])]
  transfers between devices with their start and end apart: 7 -> 8, of which waited for: 4 -> 5; matrix products, arithmetic and copies ran while one was open for 7% -> 5% of each run, Pallas kernels for 26% -> 30%
where the time goes in v3:
time: 242 us
  Pallas kernels  125 us (52%)
  waiting for transfers between devices  67.7 us (28%)
  other arithmetic  17.5 us (7%)
  between operations  13.6 us (6%)
  local copies, waits for them, and re-layouts  6.49 us (3%)
  starting transfers between devices  6.26 us (3%)
  matrix products  4.58 us (2%)
    pallas_call x1, Pallas kernels, ring_gather(): pl.pallas_call(functools.partial(ring_kernel, size), out_shape=(jax.Shape...  53.8 us
    ppermute x6, waiting for transfers between devices, swap(): return lax.ppermute(values, 'tp', [(0, 1), (1, 0)])  51.9 us
    pallas_call x3, Pallas kernels, ffn(): pl.pallas_call(ffn_kernel, grid=(count,), out_shape=jax.ShapeDtypeStruct(...  43.1 us
    pallas_call x1, Pallas kernels, mixer(): pl.pallas_call(functools.partial(mixer_kernel, paired), grid=(count,), ou...  28.5 us
    all_gather x1, waiting for transfers between devices, per_device(): ffn_all = lax.all_gather(ffn_shard, 'fs', axis=0, tiled=True)  15.3 us
    ppermute x6, starting transfers between devices, swap(): return lax.ppermute(values, 'tp', [(0, 1), (1, 0)])  6.19 us
    reduce_sum x3, other arithmetic, normed(): factor = lax.rsqrt(jnp.mean(values * values, axis=-1, keepdims=True) + EPS)  5.76 us
  transfers between devices with their start and end apart: 8, of which 5 were waited for; matrix products, arithmetic and copies ran while one was open for 5% of the time, Pallas kernels for 30%

profile of v3, /device:TPU:0, one launch (start us, length us, event | category | flops | bytes accessed | tf_op | source)
XLA Modules:
  0.0 241.6 jit_solution(11966726742180400258)
XLA Ops:
  6.5 0.0 copy-start.11
  6.5 0.0 copy-start.10
  6.5 0.0 all-gather.2.cloned.1.call-start
  6.5 2.1 fusion
  8.7 3.5 %fusion.2.x_ref = bf16[512,2048]{1,0:T(8,128)(2,1)} fusion(bf16[512,2048]{1,0:T(8,128)(2,1)} %param.15, f32[2048]{0:T(1024)} %param.16, f32[512]{0:T(512)S(1)} %add_rsqrt_fusion.3), kind=kLoop, calls=%fused_computation.8 | loop fusion | flops 4194304 | bytes 4204544 | tf_op jit(solution)/shard_map/convert_element_type | solution.py:363
  12.1 0.0 copy-done.11
  12.1 0.0 copy-done.10
  12.1 0.0 copy-done.9
  12.1 0.8 pad_maximum_fusion.3.shard_ref
  12.9 53.8 %shard_map.145 = (bf16[2048,1536]{1,0:T(8,128)(2,1)}, bf16[512,2048]{1,0:T(8,128)(2,1)}) custom-call(bf16[128,1536]{1,0:T(8,128)(2,1)} %pad_maximum_fusion.3.shard_ref, bf16[512,2048]{1,0:T(8,128)(2,1)} %fusion.2.x_ref), custom_call_target="tpu_custom_call" | custom-call | flops 4294967296 | bytes 6291456 | tf_op jit(solution)/shard_map/pallas_call | solution.py:303
  66.7 0.0 copy-done.5
  66.7 0.0 copy-done.6
  66.8 0.0 copy-done.7
  66.8 1.1 pad_maximum_fusion.1
  67.9 0.0 all-gather.2.cloned.1.call-update
  67.9 0.0 copy-start.15
  67.9 1.8 slice.21
  69.7 0.1 constant_dynamic-slice_fusion.1
  69.8 0.6 collective-permute-start
  70.4 0.0 copy-done.8
  70.4 1.0 slice_bitcast_fusion.2
  71.4 0.9 pad_maximum_fusion.2.gates_ref
  72.3 0.0 copy-done.15
  72.3 0.6 fusion.13.coef_ref
  72.9 28.5 %shard_map.146 = bf16[1024,512]{1,0:T(8,128)(2,1)} custom-call(bf16[512,2048]{1,0:T(8,128)(2,1)} %fusion.2.x_ref, bf16[512,2048]{1,0:T(8,128)(2,1)} %get-tuple-element.15.y_ref, bf16[2048,1536]{1,0:T(8,128)(2,1)} %get-tuple-element.14.wb_ref.wg_ref, bf16[2048,1536]{1,0:T(8,128)(2,1)} %get-tuple-element.14.wb_ref.wg_ref, bf16[4,512]{1,0:T(4,128)(2,1)} %conv_ref.1, ...), custom_call_target="tpu_custom_call" | custom-call | flops 12884901888 | bytes 9437184 | tf_op jit(solution)/shard_map/pallas_call | solution.py:128
  101.4 0.0 collective-permute-done
  101.4 0.1 collective-permute-start.2
  101.5 1.1 constant_dynamic-slice_fusion
  102.6 1.5 collective-permute-start.1
  104.1 0.4 collective-permute-done.2
  104.6 0.1 broadcast_select_fusion.1
  104.7 0.0 copy-start.4
  104.7 12.3 %collective-permute-done.1 = bf16[512,512]{1,0:T(8,128)(2,1)S(1)} collective-permute-done((bf16[512,512]{1,0:T(8,128)(2,1)S(1)}, bf16[512,512]{1,0:T(8,128)(2,1)S(1)}, u32[]{:S(2)}, u32[]{:S(2)}) %collective-permute-start.1) | collective-permute-done | bytes 524320 | tf_op jit(solution)/shard_map/ppermute | solution.py:330
  117.0 1.3 fusion.8
  118.3 0.0 copy-done.4
  118.3 0.0 copy-start
  118.3 0.0 copy-start.12
  118.3 3.3 %multiply_reduce_fusion.1 = (f32[512]{0:T(512)S(1)}, f32[512,2048]{1,0:T(8,128)S(1)}) fusion(f32[512,2048]{1,0:T(8,128)S(1)} %fusion.8, bf16[2048,1536]{1,0:T(8,128)(2,1)} %get-tuple-element.14.wb_ref.wg_ref, bf16[1024,512]{1,0:T(8,128)(2,1)S(1)} %copy-done.4, s32[]{:T(128)S(6)} %select_n.35), kind=kOutput, calls=%fused_computation.16 | convolution fusion | flops 1076887040 | bytes 11012100 | tf_op jit(solution)/shard_map/dot_general | solution.py:334
  121.6 0.0 copy-done
  121.7 0.0 copy-done.12
  121.7 0.0 copy-start.13
  121.7 1.0 fusion.4
  122.7 0.0 copy-done.13
  122.7 0.5 fusion.6.x_ref
  123.3 0.0 copy-start.1
  123.3 1.3 copy-done.1
  124.6 1.2 fusion.18
  125.8 1.5 collective-permute-start.3
  127.3 0.5 collective-permute-start.5
  127.8 24.0 %collective-permute-done.3.x_ref = bf16[256,2048]{1,0:T(8,128)(2,1)S(1)} collective-permute-done((bf16[256,2048]{1,0:T(8,128)(2,1)S(1)}, bf16[256,2048]{1,0:T(8,128)(2,1)S(1)}, u32[]{:S(2)}, u32[]{:S(2)}) %collective-permute-start.3) | collective-permute-done | bytes 1048608 | tf_op jit(solution)/shard_map/ppermute | solution.py:330
  151.8 15.3 %all-gather.2.cloned.1.call-done.gate_ref.up_ref.down_ref = bf16[2048,4608]{1,0:T(8,128)(2,1)} async-done(((bf16[128,4608]{1,0:T(8,128)(2,1)}), bf16[2048,4608]{1,0:T(8,128)(2,1)}) %all-gather.2.cloned.1.call-update) | async-done | bytes 18874384 | tf_op jit(solution)/shard_map/all_gather | solution.py:373
  167.2 0.0 copy-done.3
  167.2 12.7 %shard_map.148 = bf16[256,2048]{1,0:T(8,128)(2,1)} custom-call(bf16[256,2048]{1,0:T(8,128)(2,1)} %copy-done.3, bf16[2048,4608]{1,0:T(8,128)(2,1)} %all-gather.2.cloned.1.call-done.gate_ref.up_ref.down_ref, bf16[2048,4608]{1,0:T(8,128)(2,1)} %all-gather.2.cloned.1.call-done.gate_ref.up_ref.down_ref, ...), custom_call_target="tpu_custom_call" | custom-call | flops 4831838208 | bytes 20971520 | tf_op jit(solution)/shard_map/pallas_call | solution.py:180
  179.9 1.5 collective-permute-start.4
  181.3 0.0 collective-permute-done.5.x_ref
  181.3 12.7 %shard_map.149 = bf16[256,2048]{1,0:T(8,128)(2,1)} custom-call(bf16[256,2048]{1,0:T(8,128)(2,1)} %collective-permute-done.5.x_ref, bf16[2048,4608]{1,0:T(8,128)(2,1)} %all-gather.2.cloned.1.call-done.gate_ref.up_ref.down_ref, bf16[2048,4608]{1,0:T(8,128)(2,1)} %all-gather.2.cloned.1.call-done.gate_ref.up_ref.down_ref, ...), custom_call_target="tpu_custom_call" | custom-call | flops 4831838208 | bytes 20971520 | tf_op jit(solution)/shard_map/pallas_call | solution.py:180
  194.1 0.6 collective-permute-start.6
  194.6 17.7 %shard_map.147 = bf16[512,2048]{1,0:T(8,128)(2,1)} custom-call(bf16[512,2048]{1,0:T(8,128)(2,1)} %copy-done.1, bf16[2048,4608]{1,0:T(8,128)(2,1)} %all-gather.2.cloned.1.call-done.gate_ref.up_ref.down_ref, bf16[2048,4608]{1,0:T(8,128)(2,1)} %all-gather.2.cloned.1.call-done.gate_ref.up_ref.down_ref, ...), custom_call_target="tpu_custom_call" | custom-call | flops 9663676416 | bytes 23068672 | tf_op jit(solution)/shard_map/pallas_call | solution.py:180
  212.3 0.0 collective-permute-done.4
  212.3 15.6 %collective-permute-done.6 = bf16[256,2048]{1,0:T(8,128)(2,1)} collective-permute-done((bf16[256,2048]{1,0:T(8,128)(2,1)}, bf16[256,2048]{1,0:T(8,128)(2,1)}, u32[]{:S(2)}, u32[]{:S(2)}) %collective-permute-start.6) | collective-permute-done | bytes 1048608 | tf_op jit(solution)/shard_map/ppermute | solution.py:330
  228.0 2.6 %multiply_reduce_fusion = f32[512]{0:T(512)S(1)} fusion(bf16[512,2048]{1,0:T(8,128)(2,1)} %shard_map.147, bf16[256,2048]{1,0:T(8,128)(2,1)} %collective-permute-done.6, bf16[256,2048]{1,0:T(8,128)(2,1)S(1)} %collective-permute-done.4), kind=kLoop, calls=%fused_computation.14 | loop fusion | flops 8388096 | bytes 4196352 | tf_op jit(solution)/shard_map/reduce_sum | solution.py:17
  230.6 0.0 copy-done.2
  230.6 0.0 copy-done.14
  230.6 4.2 %fusion.7 = bf16[512,2048]{1,0:T(8,128)(2,1)} fusion(bf16[512,2048]{1,0:T(8,128)(2,1)S(1)} %get-tuple-element.20, bf16[512,2048]{1,0:T(8,128)(2,1)S(1)} %copy-done.2, f32[2048]{0:T(1024)S(1)} %copy-done.14, f32[512]{0:T(512)S(1)} %add_rsqrt_fusion, bf16[256,2048]{1,0:T(8,128)(2,1)} %collective-permute-done.6, bf16[256,2048]{1,0:T(8,128)(2,1)S(1)} %collective-permute-done.4), kind=kLoop, calls=%fused_computation.13 | loop fusion | flops 11534336 | bytes 8398848 | tf_op jit(solution)/shard_map/convert_element_type | solution.py:412
  (12 shorter events, 0.0 us)
Async XLA Ops:
  6.5 5.6 %copy-start.11 = (bf16[128,512]{1,0:T(8,128)(2,1)S(1)}, bf16[128,512]{1,0:T(8,128)(2,1)}, u32[]{:S(2)}) copy-start(bf16[128,512]{1,0:T(8,128)(2,1)} %param.20) | copy-start | bytes 393220
  6.5 5.6 %copy-start.10 = (bf16[128,512]{1,0:T(8,128)(2,1)S(1)}, bf16[128,512]{1,0:T(8,128)(2,1)}, u32[]{:S(2)}) copy-start(bf16[128,512]{1,0:T(8,128)(2,1)} %param.21) | copy-start | bytes 393220
  6.5 5.6 %copy-start.9 = (bf16[128,512]{1,0:T(8,128)(2,1)S(1)}, bf16[128,512]{1,0:T(8,128)(2,1)}, u32[]{:S(2)}) copy-start(bf16[128,512]{1,0:T(8,128)(2,1)} %param.26) | copy-start | bytes 393220
  6.5 160.6 %all-gather.2.cloned.1.call-start = ((), (), s32[]{:S(2)}) async-start(), calls=%async_computation | async-start | bytes 20054016 | tf_op jit(solution)/shard_map/all_gather | solution.py:373
  12.9 53.8 %copy-start.5 = (bf16[128,1536]{1,0:T(8,128)(2,1)S(1)}, bf16[128,1536]{1,0:T(8,128)(2,1)}, u32[]{:S(2)}) copy-start(bf16[128,1536]{1,0:T(8,128)(2,1)} %param.29) | copy-start | bytes 1179652
  12.9 53.8 %copy-start.6 = (bf16[128,1536]{1,0:T(8,128)(2,1)S(1)}, bf16[128,1536]{1,0:T(8,128)(2,1)}, u32[]{:S(2)}) copy-start(bf16[128,1536]{1,0:T(8,128)(2,1)} %param.28) | copy-start | bytes 1179652
  12.9 53.8 %copy-start.7 = (bf16[128,1536]{1,0:T(8,128)(2,1)S(1)}, bf16[128,1536]{1,0:T(8,128)(2,1)}, u32[]{:S(2)}) copy-start(bf16[128,1536]{1,0:T(8,128)(2,1)} %param.27) | copy-start | bytes 1179652
  67.9 2.5 %copy-start.8 = (bf16[2,4,128,128]{3,2,1,0:T(8,128)(2,1)S(1)}, bf16[2,4,128,128]{3,2,1,0:T(8,128)(2,1)}, u32[]{:S(2)}) copy-start(bf16[2,4,128,128]{3,2,1,0:T(8,128)(2,1)} %param.24) | copy-start | bytes 786436
  67.9 4.4 %copy-start.15 = (f32[2,512]{1,0:T(2,128)S(1)}, f32[2,512]{1,0:T(2,128)}, u32[]{:S(2)}) copy-start(f32[2,512]{1,0:T(2,128)} %param.25) | copy-start | bytes 12292
  69.8 31.7 %collective-permute-start = (bf16[1024,512]{1,0:T(8,128)(2,1)S(1)}, bf16[1024,512]{1,0:T(8,128)(2,1)S(1)}, u32[]{:S(2)}, u32[]{:S(2)}) collective-permute-start(bf16[1024,512]{1,0:T(8,128)(2,1)S(1)} %constant_dynamic-slice_fusion.1), channel_id=1, source_target_pairs={{0,1},{1,0},{2,3},{3,2},{4,5},{5,4},{6,7},{7,6},{8,9},{9,8},{10,11... | collective-permute-start | bytes 3145736 | tf_op jit(solution)/shard_map/ppermute | solution.py:330
  101.4 3.1 %collective-permute-start.2 = (bf16[1024,512]{1,0:T(8,128)(2,1)S(1)}, bf16[1024,512]{1,0:T(8,128)(2,1)S(1)}, u32[]{:S(2)}, u32[]{:S(2)}) collective-permute-start(bf16[1024,512]{1,0:T(8,128)(2,1)S(1)} %collective-permute-done), channel_id=1, source_target_pairs={{0,2},{2,0},{4,6},{6,4},{8,10},{10,8},{12,14},{14,12},{16,18},{18,... | collective-permute-start | bytes 3145736 | tf_op jit(solution)/shard_map/ppermute | solution.py:383
  102.6 14.4 %collective-permute-start.1 = (bf16[512,512]{1,0:T(8,128)(2,1)S(1)}, bf16[512,512]{1,0:T(8,128)(2,1)S(1)}, u32[]{:S(2)}, u32[]{:S(2)}) collective-permute-start(bf16[512,512]{1,0:T(8,128)(2,1)S(1)} %constant_dynamic-slice_fusion), channel_id=1, source_target_pairs={{0,1},{1,0},{2,3},{3,2},{4,5},{5,4},{6,7},{7,6},{8,9},{9,8},{10,11... | collective-permute-start | bytes 1572872 | tf_op jit(solution)/shard_map/ppermute | solution.py:330
  104.7 13.6 %copy-start.4 = (bf16[1024,512]{1,0:T(8,128)(2,1)S(1)}, bf16[1024,512]{1,0:T(8,128)(2,1)}, u32[]{:S(2)}) copy-start(bf16[1024,512]{1,0:T(8,128)(2,1)} %shard_map.146) | copy-start | bytes 3145732
  118.3 3.3 %copy-start = (bf16[512,2048]{1,0:T(8,128)(2,1)S(1)}, bf16[512,2048]{1,0:T(8,128)(2,1)}, u32[]{:S(2)}) copy-start(bf16[512,2048]{1,0:T(8,128)(2,1)} %param.15) | copy-start | bytes 6291460
  118.3 3.3 %copy-start.12 = (f32[2048]{0:T(1024)S(1)}, f32[2048]{0:T(1024)}, u32[]{:S(2)}) copy-start(f32[2048]{0:T(1024)} %param.17) | copy-start | bytes 24580
  121.7 1.1 copy-start.13
  123.3 1.3 copy-start.1
  125.8 26.0 %collective-permute-start.3 = (bf16[256,2048]{1,0:T(8,128)(2,1)S(1)}, bf16[256,2048]{1,0:T(8,128)(2,1)S(1)}, u32[]{:S(2)}, u32[]{:S(2)}) collective-permute-start(bf16[256,2048]{1,0:T(8,128)(2,1)S(1)} %get-tuple-element.21), channel_id=1, source_target_pairs={{0,1},{1,0},{2,3},{3,2},{4,5},{5,4},{6,7},{7,6},{8,9},{9,8},{10,11... | collective-permute-start | bytes 3145736 | tf_op jit(solution)/shard_map/ppermute | solution.py:330
  127.3 54.1 %collective-permute-start.5 = (bf16[256,2048]{1,0:T(8,128)(2,1)}, bf16[256,2048]{1,0:T(8,128)(2,1)}, u32[]{:S(2)}, u32[]{:S(2)}) collective-permute-start(bf16[256,2048]{1,0:T(8,128)(2,1)} %get-tuple-element.22), channel_id=1, source_target_pairs={{0,1},{1,0},{2,3},{3,2},{4,5},{5,4},{6,7},{7,6},{8,9},{9,8},{10,11... | collective-permute-start | bytes 3145736 | tf_op jit(solution)/shard_map/ppermute | solution.py:330
  151.8 15.3 %copy-start.3 = (bf16[256,2048]{1,0:T(8,128)(2,1)}, bf16[256,2048]{1,0:T(8,128)(2,1)S(1)}, u32[]{:S(2)}) copy-start(bf16[256,2048]{1,0:T(8,128)(2,1)S(1)} %collective-permute-done.3.x_ref) | copy-start | bytes 3145732
  179.9 32.5 %collective-permute-start.4 = (bf16[256,2048]{1,0:T(8,128)(2,1)}, bf16[256,2048]{1,0:T(8,128)(2,1)S(1)}, u32[]{:S(2)}, u32[]{:S(2)}) collective-permute-start(bf16[256,2048]{1,0:T(8,128)(2,1)} %shard_map.148), channel_id=1, source_target_pairs={{0,1},{1,0},{2,3},{3,2},{4,5},{5,4},{6,7},{7,6},{8,9},{9,8},{10,11... | collective-permute-start | bytes 3145736 | tf_op jit(solution)/shard_map/ppermute | solution.py:330
  194.1 33.9 %collective-permute-start.6 = (bf16[256,2048]{1,0:T(8,128)(2,1)}, bf16[256,2048]{1,0:T(8,128)(2,1)}, u32[]{:S(2)}, u32[]{:S(2)}) collective-permute-start(bf16[256,2048]{1,0:T(8,128)(2,1)} %shard_map.149), channel_id=1, source_target_pairs={{0,1},{1,0},{2,3},{3,2},{4,5},{5,4},{6,7},{7,6},{8,9},{9,8},{10,11... | collective-permute-start | bytes 3145736 | tf_op jit(solution)/shard_map/ppermute | solution.py:330
  212.3 18.3 %copy-start.2 = (bf16[512,2048]{1,0:T(8,128)(2,1)S(1)}, bf16[512,2048]{1,0:T(8,128)(2,1)}, u32[]{:S(2)}) copy-start(bf16[512,2048]{1,0:T(8,128)(2,1)} %shard_map.147) | copy-start | bytes 6291460
  212.3 18.3 %copy-start.14 = (f32[2048]{0:T(1024)S(1)}, f32[2048]{0:T(1024)}, u32[]{:S(2)}) copy-start(f32[2048]{0:T(1024)} %param.19) | copy-start | bytes 24580
Sparse Core Ops, SparseCore 0:
  68.0 99.0 all-gather.1

commit v4 on v3

--- a/solution.py
+++ b/solution.py
@@ -10,6 +10,7 @@
 EPS = 1e-06
 SEGMENTS = 8
 PIECES = 4
+ROW_BLOCK = 64
 VMEM_BYTES = 60 * 1024 * 1024
 
 
@@ -324,6 +325,44 @@
             flops=1 << 32, bytes_accessed=2 * rows * size * width, transcendentals=0
         ),
     )(shard, x)
+
+
+def finish_kernel(middle_ref, own_ref, back_ref, gain_ref, *rest):
+    out_ref = rest[-1]
+    ffn_sum = own_ref[...].astype(jnp.float32) + back_ref[...].astype(jnp.float32)
+    out_ref[...] = (
+        middle_ref[...].astype(jnp.float32) + normed(ffn_sum, gain_ref[...])
+    ).astype(jnp.bfloat16)
+
+
+def finish(middle, own, back, gain, start, done):
+    model = middle.shape[1]
+    rows = ROW_BLOCK
+    first = start // rows
+    placed = pl.BlockSpec((rows, model), lambda i: (first + i, 0))
+    operands = [middle, own, back, gain.reshape(1, model)]
+    specs = [
+        placed,
+        placed,
+        pl.BlockSpec((rows, model), lambda i: (i, 0)),
+        pl.BlockSpec((1, model), lambda i: (0, 0)),
+    ]
+    aliases = {}
+    if done is not None:
+        aliases = {len(operands): 0}
+        operands.append(done)
+        specs.append(pl.BlockSpec(memory_space=pl.ANY))
+    return pl.pallas_call(
+        finish_kernel,
+        grid=(back.shape[0] // rows,),
+        out_shape=jax.ShapeDtypeStruct(middle.shape, jnp.bfloat16),
+        in_specs=specs,
+        out_specs=placed,
+        input_output_aliases=aliases,
+        cost_estimate=pl.CostEstimate(
+            flops=8 * back.size, bytes_accessed=8 * back.size, transcendentals=0
+        ),
+    )(*operands)
 
 
 def swap(values):
@@ -398,12 +437,26 @@
     middle = residual.astype(jnp.float32)
     normed_mid = normed(middle, pre_ffn_gain).astype(jnp.bfloat16)
     if pair:
-        pieces = 2
-        size = own_rows // pieces
-        away_rows = [swap(normed_mid[i * size : (i + 1) * size]) for i in range(pieces)]
-        back = [swap(ffn(rows, ffn_all)) for rows in away_rows]
-        own_part = ffn(normed_mid, ffn_all).astype(jnp.float32)
-        ffn_sum = own_part + jnp.concatenate(back, axis=0).astype(jnp.float32)
+        blocks = own_rows // ROW_BLOCK
+        cuts = [0, blocks // 4, blocks // 4 + 3 * blocks // 8, blocks]
+        spans = [(i * ROW_BLOCK, j * ROW_BLOCK) for i, j in zip(cuts, cuts[1:])]
+        away_rows, partials = [], []
+        for start, end in spans:
+            rows = normed_mid[start:end]
+            if away_rows:
+                rows, away_rows[-1] = lax.optimization_barrier((rows, away_rows[-1]))
+            away_rows.append(swap(rows))
+        for rows in away_rows:
+            if partials:
+                rows, partials[-1] = lax.optimization_barrier((rows, partials[-1]))
+            partials.append(ffn(rows, ffn_all))
+        normed_mid, partials[-1] = lax.optimization_barrier((normed_mid, partials[-1]))
+        back = [swap(partial) for partial in partials]
+        own_part = ffn(normed_mid, ffn_all)
+        done = None
+        for (start, end), came in zip(spans, back):
+            done = finish(residual, own_part, came, post_ffn_gain, start, done)
+        return done
     else:
         all_mid = lax.all_gather(normed_mid, "tp", axis=0, tiled=True)
         ffn_sum = lax.psum_scatter(

time: 242 us -> 263 us (1.087)
  Pallas kernels: 125 us -> 145 us
  other arithmetic: 17.5 us -> 10.7 us
  starting transfers between devices: 6.26 us -> 10.2 us
  waiting for transfers between devices: 67.7 us -> 70.9 us
    pallas_call x3 -> x4, Pallas kernels: 43.1 us -> 53.2 us  [ffn(): pl.pallas_call(ffn_kernel, grid=(count,), out_shape=jax.ShapeDtypeStruct(...]
    pallas_call x0 -> x3, Pallas kernels: none -> 9.33 us  [finish(): pl.pallas_call(finish_kernel, grid=(back.shape[0] // rows,), out_shape=ja...]
    ppermute x6 -> x8, waiting for transfers between devices: 51.9 us -> 59.9 us  [swap(): return lax.ppermute(values, 'tp', [(0, 1), (1, 0)])]
    all_gather x1, waiting for transfers between devices: 15.3 us -> 10.5 us  [per_device(): ffn_all = lax.all_gather(ffn_shard, 'fs', axis=0, tiled=True)]
    convert_element_type x1 -> x0, other arithmetic: 4.17 us -> none  [per_device(): return (middle + normed(ffn_sum, post_ffn_gain)).astype(jnp.bfloat16)]
    ppermute x6 -> x8, starting transfers between devices: 6.19 us -> 10.2 us  [swap(): return lax.ppermute(values, 'tp', [(0, 1), (1, 0)])]
    reduce_sum x3 -> x2, other arithmetic: 5.76 us -> 3.15 us  [normed(): factor = lax.rsqrt(jnp.mean(values * values, axis=-1, keepdims=True) + EPS)]
  transfers between devices with their start and end apart: 8 -> 10, of which waited for: 5 -> 7; matrix products, arithmetic and copies ran while one was open for 5% -> 5% of each run, Pallas kernels for 30% -> 29%
where the time goes in v4:
time: 263 us
  Pallas kernels  145 us (55%)
  waiting for transfers between devices  70.9 us (27%)
  between operations  13.7 us (5%)
  other arithmetic  10.7 us (4%)
  starting transfers between devices  10.2 us (4%)
  local copies, waits for them, and re-layouts  7.75 us (3%)
  matrix products  4.53 us (2%)
    ppermute x8, waiting for transfers between devices, swap(): return lax.ppermute(values, 'tp', [(0, 1), (1, 0)])  59.9 us
    pallas_call x1, Pallas kernels, ring_gather(): pl.pallas_call(functools.partial(ring_kernel, size), out_shape=(jax.Shape...  53.8 us
    pallas_call x4, Pallas kernels, ffn(): pl.pallas_call(ffn_kernel, grid=(count,), out_shape=jax.ShapeDtypeStruct(...  53.2 us
    pallas_call x1, Pallas kernels, mixer(): pl.pallas_call(functools.partial(mixer_kernel, paired), grid=(count,), ou...  28.5 us
    all_gather x1, waiting for transfers between devices, per_device(): ffn_all = lax.all_gather(ffn_shard, 'fs', axis=0, tiled=True)  10.5 us
    ppermute x8, starting transfers between devices, swap(): return lax.ppermute(values, 'tp', [(0, 1), (1, 0)])  10.2 us
    pallas_call x3, Pallas kernels, finish(): pl.pallas_call(finish_kernel, grid=(back.shape[0] // rows,), out_shape=ja...  9.33 us
  transfers between devices with their start and end apart: 10, of which 7 were waited for; matrix products, arithmetic and copies ran while one was open for 5% of the time, Pallas kernels for 29%

profile of v4, /device:TPU:0, one launch (start us, length us, event | category | flops | bytes accessed | tf_op | source)
XLA Modules:
  0.0 262.6 jit_solution(16875751171790417540)
XLA Ops:
  6.5 0.0 all-gather.2.cloned.1.call-start
  6.5 2.1 fusion.3
  8.7 3.5 %fusion.5.x_ref = bf16[512,2048]{1,0:T(8,128)(2,1)} fusion(bf16[512,2048]{1,0:T(8,128)(2,1)} %param.15, f32[2048]{0:T(1024)} %param.16, f32[512]{0:T(512)S(1)} %add_rsqrt_fusion.2), kind=kLoop, calls=%fused_computation.10 | loop fusion | flops 4194304 | bytes 4204544 | tf_op jit(solution)/shard_map/convert_element_type | solution.py:402
  12.1 0.0 copy-done.18
  12.1 0.0 copy-done.17
  12.1 0.0 copy-done.16
  12.1 0.8 pad_maximum_fusion.2.shard_ref
  12.9 53.8 %shard_map.145 = (bf16[2048,1536]{1,0:T(8,128)(2,1)}, bf16[512,2048]{1,0:T(8,128)(2,1)}) custom-call(bf16[128,1536]{1,0:T(8,128)(2,1)} %pad_maximum_fusion.2.shard_ref, bf16[512,2048]{1,0:T(8,128)(2,1)} %fusion.5.x_ref), custom_call_target="tpu_custom_call" | custom-call | flops 4294967296 | bytes 6291456 | tf_op jit(solution)/shard_map/pallas_call | solution.py:304
  66.7 0.0 copy-done.12
  66.8 0.0 copy-done.13
  66.8 1.1 pad_maximum_fusion
  67.9 0.0 all-gather.2.cloned.1.call-update
  67.9 0.0 copy-start.21
  67.9 1.8 slice.24
  69.7 0.1 constant_dynamic-slice_fusion.1
  69.8 0.6 collective-permute-start
  70.4 1.0 slice_bitcast_fusion.2
  71.4 0.9 pad_maximum_fusion.1.gates_ref
  72.3 0.0 copy-done.21
  72.3 0.6 fusion.12.coef_ref
  72.9 28.5 %shard_map.146 = bf16[1024,512]{1,0:T(8,128)(2,1)} custom-call(bf16[512,2048]{1,0:T(8,128)(2,1)} %fusion.5.x_ref, bf16[512,2048]{1,0:T(8,128)(2,1)} %get-tuple-element.25.y_ref, bf16[2048,1536]{1,0:T(8,128)(2,1)} %get-tuple-element.24.wb_ref.wg_ref, bf16[2048,1536]{1,0:T(8,128)(2,1)} %get-tuple-element.24.wb_ref.wg_ref, bf16[4,512]{1,0:T(4,128)(2,1)} %conv_ref.1, ...), custom_call_target="tpu_custom_call" | custom-call | flops 12884901888 | bytes 9437184 | tf_op jit(solution)/shard_map/pallas_call | solution.py:129
  101.4 0.0 collective-permute-done
  101.4 0.1 collective-permute-start.2
  101.5 1.1 constant_dynamic-slice_fusion
  102.6 1.5 collective-permute-start.1
  104.1 0.4 collective-permute-done.2
  104.5 0.1 broadcast_select_fusion.1
  104.7 12.2 %collective-permute-done.1 = bf16[512,512]{1,0:T(8,128)(2,1)S(1)} collective-permute-done((bf16[512,512]{1,0:T(8,128)(2,1)S(1)}, bf16[512,512]{1,0:T(8,128)(2,1)S(1)}, u32[]{:S(2)}, u32[]{:S(2)}) %collective-permute-start.1) | collective-permute-done | bytes 524320 | tf_op jit(solution)/shard_map/ppermute | solution.py:369
  116.9 1.3 fusion.7
  118.2 0.0 copy-start.1
  118.3 0.0 copy-start.19
  118.3 3.3 %multiply_reduce_fusion = (f32[512]{0:T(512)S(1)}, f32[512,2048]{1,0:T(8,128)S(1)}) fusion(f32[512,2048]{1,0:T(8,128)S(1)} %fusion.7, bf16[2048,1536]{1,0:T(8,128)(2,1)} %get-tuple-element.24.wb_ref.wg_ref, bf16[1024,512]{1,0:T(8,128)(2,1)S(1)} %copy-done.3, s32[]{:T(128)S(6)} %select_n.35), kind=kOutput, calls=%fused_computation.12 | convolution fusion | flops 1076887040 | bytes 11012100 | tf_op jit(solution)/shard_map/dot_general | solution.py:373
  121.5 0.0 copy-start.20
  121.6 1.0 fusion
  122.6 0.6 fusion.2.x_ref
  123.2 0.0 copy-start.2
  123.2 1.5 collective-permute-start.3
  124.8 0.2 fusion.17
  125.0 11.8 %collective-permute-done.3.x_ref = bf16[128,2048]{1,0:T(8,128)(2,1)S(1)} collective-permute-done((bf16[128,2048]{1,0:T(8,128)(2,1)S(1)}, bf16[128,2048]{1,0:T(8,128)(2,1)S(1)}, u32[]{:S(2)}, u32[]{:S(2)}) %collective-permute-start.3) | collective-permute-done | bytes 524320 | tf_op jit(solution)/shard_map/ppermute | solution.py:369
  136.8 0.0 copy-done.2
  136.8 1.5 collective-permute-start.4
  138.3 16.9 %collective-permute-done.4.x_ref = bf16[192,2048]{1,0:T(8,128)(2,1)S(1)} collective-permute-done((bf16[192,2048]{1,0:T(8,128)(2,1)S(1)}, bf16[192,2048]{1,0:T(8,128)(2,1)S(1)}, u32[]{:S(2)}, u32[]{:S(2)}) %collective-permute-start.4) | collective-permute-done | bytes 786464 | tf_op jit(solution)/shard_map/ppermute | solution.py:369
  155.1 1.5 collective-permute-start.5
  156.6 10.5 %all-gather.2.cloned.1.call-done.gate_ref.up_ref.down_ref = bf16[2048,4608]{1,0:T(8,128)(2,1)} async-done(((bf16[128,4608]{1,0:T(8,128)(2,1)}), bf16[2048,4608]{1,0:T(8,128)(2,1)}) %all-gather.2.cloned.1.call-update) | async-done | bytes 18874384 | tf_op jit(solution)/shard_map/all_gather | solution.py:412
  167.1 11.1 %shard_map.147 = bf16[128,2048]{1,0:T(8,128)(2,1)} custom-call(bf16[128,2048]{1,0:T(8,128)(2,1)} %copy-done.9, bf16[2048,4608]{1,0:T(8,128)(2,1)} %all-gather.2.cloned.1.call-done.gate_ref.up_ref.down_ref, bf16[2048,4608]{1,0:T(8,128)(2,1)} %all-gather.2.cloned.1.call-done.gate_ref.up_ref.down_ref, ...), custom_call_target="tpu_custom_call" | custom-call | flops 2415919104 | bytes 19922944 | tf_op jit(solution)/shard_map/pallas_call | solution.py:181
  178.3 0.0 copy-done.5
  178.3 12.3 %shard_map.148 = bf16[192,2048]{1,0:T(8,128)(2,1)} custom-call(bf16[192,2048]{1,0:T(8,128)(2,1)} %copy-done.5, bf16[2048,4608]{1,0:T(8,128)(2,1)} %all-gather.2.cloned.1.call-done.gate_ref.up_ref.down_ref, bf16[2048,4608]{1,0:T(8,128)(2,1)} %all-gather.2.cloned.1.call-done.gate_ref.up_ref.down_ref, ...), custom_call_target="tpu_custom_call" | custom-call | flops 3623878656 | bytes 20447232 | tf_op jit(solution)/shard_map/pallas_call | solution.py:181
  190.6 0.0 collective-permute-done.5.x_ref
  190.6 0.9 copy-done.6
  191.5 12.0 %shard_map.149 = bf16[192,2048]{1,0:T(8,128)(2,1)} custom-call(bf16[192,2048]{1,0:T(8,128)(2,1)} %copy-done.6, bf16[2048,4608]{1,0:T(8,128)(2,1)} %all-gather.2.cloned.1.call-done.gate_ref.up_ref.down_ref, bf16[2048,4608]{1,0:T(8,128)(2,1)} %all-gather.2.cloned.1.call-done.gate_ref.up_ref.down_ref, ...), custom_call_target="tpu_custom_call" | custom-call | flops 3623878656 | bytes 20447232 | tf_op jit(solution)/shard_map/pallas_call | solution.py:181
  203.5 1.5 collective-permute-start.8
  205.0 0.0 copy-done.4
  205.0 0.6 collective-permute-start.7
  205.6 1.5 collective-permute-start.6
  207.0 17.8 %shard_map.150.own_ref = bf16[512,2048]{1,0:T(8,128)(2,1)} custom-call(bf16[512,2048]{1,0:T(8,128)(2,1)} %copy-done.2, bf16[2048,4608]{1,0:T(8,128)(2,1)} %all-gather.2.cloned.1.call-done.gate_ref.up_ref.down_ref, bf16[2048,4608]{1,0:T(8,128)(2,1)} %all-gather.2.cloned.1.call-done.gate_ref.up_ref.down_ref, ...), custom_call_target="tpu_custom_call" | custom-call | flops 9663676416 | bytes 23068672 | tf_op jit(solution)/shard_map/pallas_call | solution.py:181
  224.8 0.0 collective-permute-done.8.back_ref
  224.8 0.8 copy-done.11
  225.6 2.3 shard_map.151.rest_0_
  227.9 7.3 %collective-permute-done.7.back_ref = bf16[192,2048]{1,0:T(8,128)(2,1)S(1)} collective-permute-done((bf16[192,2048]{1,0:T(8,128)(2,1)S(1)}, bf16[192,2048]{1,0:T(8,128)(2,1)S(1)}, u32[]{:S(2)}, u32[]{:S(2)}) %collective-permute-start.7) | collective-permute-done | bytes 786464 | tf_op jit(solution)/shard_map/ppermute | solution.py:369
  235.2 0.9 copy-done.8
  236.1 3.5 %shard_map.152.rest_0_ = bf16[512,2048]{1,0:T(8,128)(2,1)} custom-call(bf16[512,2048]{1,0:T(8,128)(2,1)} %copy-done, bf16[512,2048]{1,0:T(8,128)(2,1)} %shard_map.150.own_ref, bf16[192,2048]{1,0:T(8,128)(2,1)} %copy-done.8, f32[1,2048]{1,0:T(1,128)} %bitcast.11, bf16[512,2048]{1,0:T(8,128)(2,1)} %shard_map.151.rest_0_), custom_call_target="tpu_custom_call", output_to_operand_aliasing={{}: (4, {})} | custom-call | flops 3145728 | bytes 3145728 | tf_op jit(solution)/shard_map/pallas_call | solution.py:355
  239.6 11.7 %collective-permute-done.6.back_ref = bf16[192,2048]{1,0:T(8,128)(2,1)S(1)} collective-permute-done((bf16[192,2048]{1,0:T(8,128)(2,1)}, bf16[192,2048]{1,0:T(8,128)(2,1)S(1)}, u32[]{:S(2)}, u32[]{:S(2)}) %collective-permute-start.6) | collective-permute-done | bytes 786464 | tf_op jit(solution)/shard_map/ppermute | solution.py:369
  251.3 0.9 copy-done.7
  252.2 3.5 %shard_map.153 = bf16[512,2048]{1,0:T(8,128)(2,1)} custom-call(bf16[512,2048]{1,0:T(8,128)(2,1)} %copy-done, bf16[512,2048]{1,0:T(8,128)(2,1)} %shard_map.150.own_ref, bf16[192,2048]{1,0:T(8,128)(2,1)} %copy-done.7, f32[1,2048]{1,0:T(1,128)} %bitcast.12, bf16[512,2048]{1,0:T(8,128)(2,1)} %shard_map.152.rest_0_), custom_call_target="tpu_custom_call", output_to_operand_aliasing={{}: (4, {})} | custom-call | flops 3145728 | bytes 3145728 | tf_op jit(solution)/shard_map/pallas_call | solution.py:355
  (30 shorter events, 0.1 us)
Async XLA Ops:
  6.5 5.6 %copy-start.18 = (bf16[128,512]{1,0:T(8,128)(2,1)S(1)}, bf16[128,512]{1,0:T(8,128)(2,1)}, u32[]{:S(2)}) copy-start(bf16[128,512]{1,0:T(8,128)(2,1)} %param.20) | copy-start | bytes 393220
  6.5 5.6 %copy-start.17 = (bf16[128,512]{1,0:T(8,128)(2,1)S(1)}, bf16[128,512]{1,0:T(8,128)(2,1)}, u32[]{:S(2)}) copy-start(bf16[128,512]{1,0:T(8,128)(2,1)} %param.21) | copy-start | bytes 393220
  6.5 5.6 %copy-start.16 = (bf16[128,512]{1,0:T(8,128)(2,1)S(1)}, bf16[128,512]{1,0:T(8,128)(2,1)}, u32[]{:S(2)}) copy-start(bf16[128,512]{1,0:T(8,128)(2,1)} %param.26) | copy-start | bytes 393220
  6.5 160.6 %all-gather.2.cloned.1.call-start = ((), (), s32[]{:S(2)}) async-start(), calls=%async_computation | async-start | bytes 20054016 | tf_op jit(solution)/shard_map/all_gather | solution.py:412
  12.9 53.8 %copy-start.12 = (bf16[128,1536]{1,0:T(8,128)(2,1)S(1)}, bf16[128,1536]{1,0:T(8,128)(2,1)}, u32[]{:S(2)}) copy-start(bf16[128,1536]{1,0:T(8,128)(2,1)} %param.29) | copy-start | bytes 1179652
  12.9 53.8 %copy-start.13 = (bf16[128,1536]{1,0:T(8,128)(2,1)S(1)}, bf16[128,1536]{1,0:T(8,128)(2,1)}, u32[]{:S(2)}) copy-start(bf16[128,1536]{1,0:T(8,128)(2,1)} %param.28) | copy-start | bytes 1179652
  12.9 53.8 %copy-start.14 = (bf16[128,1536]{1,0:T(8,128)(2,1)S(1)}, bf16[128,1536]{1,0:T(8,128)(2,1)}, u32[]{:S(2)}) copy-start(bf16[128,1536]{1,0:T(8,128)(2,1)} %param.27) | copy-start | bytes 1179652
  67.9 2.5 copy-start.15
  67.9 4.4 %copy-start.21 = (f32[2,512]{1,0:T(2,128)S(1)}, f32[2,512]{1,0:T(2,128)}, u32[]{:S(2)}) copy-start(f32[2,512]{1,0:T(2,128)} %param.25) | copy-start | bytes 12292
  69.8 31.6 %collective-permute-start = (bf16[1024,512]{1,0:T(8,128)(2,1)S(1)}, bf16[1024,512]{1,0:T(8,128)(2,1)S(1)}, u32[]{:S(2)}, u32[]{:S(2)}) collective-permute-start(bf16[1024,512]{1,0:T(8,128)(2,1)S(1)} %constant_dynamic-slice_fusion.1), channel_id=1, source_target_pairs={{0,1},{1,0},{2,3},{3,2},{4,5},{5,4},{6,7},{7,6},{8,9},{9,8},{10,11... | collective-permute-start | bytes 3145736 | tf_op jit(solution)/shard_map/ppermute | solution.py:369
  101.4 3.1 %collective-permute-start.2 = (bf16[1024,512]{1,0:T(8,128)(2,1)S(1)}, bf16[1024,512]{1,0:T(8,128)(2,1)S(1)}, u32[]{:S(2)}, u32[]{:S(2)}) collective-permute-start(bf16[1024,512]{1,0:T(8,128)(2,1)S(1)} %collective-permute-done), channel_id=1, source_target_pairs={{0,2},{2,0},{4,6},{6,4},{8,10},{10,8},{12,14},{14,12},{16,18},{18,... | collective-permute-start | bytes 3145736 | tf_op jit(solution)/shard_map/ppermute | solution.py:422
  102.6 14.4 %collective-permute-start.1 = (bf16[512,512]{1,0:T(8,128)(2,1)S(1)}, bf16[512,512]{1,0:T(8,128)(2,1)S(1)}, u32[]{:S(2)}, u32[]{:S(2)}) collective-permute-start(bf16[512,512]{1,0:T(8,128)(2,1)S(1)} %constant_dynamic-slice_fusion), channel_id=1, source_target_pairs={{0,1},{1,0},{2,3},{3,2},{4,5},{5,4},{6,7},{7,6},{8,9},{9,8},{10,11... | collective-permute-start | bytes 1572872 | tf_op jit(solution)/shard_map/ppermute | solution.py:369
  104.7 13.5 %copy-start.3 = (bf16[1024,512]{1,0:T(8,128)(2,1)S(1)}, bf16[1024,512]{1,0:T(8,128)(2,1)}, u32[]{:S(2)}) copy-start(bf16[1024,512]{1,0:T(8,128)(2,1)} %shard_map.146) | copy-start | bytes 3145732
  118.2 3.3 %copy-start.1 = (bf16[512,2048]{1,0:T(8,128)(2,1)S(1)}, bf16[512,2048]{1,0:T(8,128)(2,1)}, u32[]{:S(2)}) copy-start(bf16[512,2048]{1,0:T(8,128)(2,1)} %param.15) | copy-start | bytes 6291460
  118.3 3.3 %copy-start.19 = (f32[2048]{0:T(1024)S(1)}, f32[2048]{0:T(1024)}, u32[]{:S(2)}) copy-start(f32[2048]{0:T(1024)} %param.17) | copy-start | bytes 24580
  121.5 1.1 copy-start.20
  122.6 2.4 copy-start
  123.2 13.6 %copy-start.2 = (bf16[512,2048]{1,0:T(8,128)(2,1)}, bf16[512,2048]{1,0:T(8,128)(2,1)S(1)}, u32[]{:S(2)}) copy-start(bf16[512,2048]{1,0:T(8,128)(2,1)S(1)} %fusion.2.x_ref) | copy-start | bytes 6291460
  123.2 13.5 %collective-permute-start.3 = (bf16[128,2048]{1,0:T(8,128)(2,1)S(1)}, bf16[128,2048]{1,0:T(8,128)(2,1)S(1)}, u32[]{:S(2)}, u32[]{:S(2)}) collective-permute-start(bf16[128,2048]{1,0:T(8,128)(2,1)S(1)} %slice.34), channel_id=1, source_target_pairs={{0,1},{1,0},{2,3},{3,2},{4,5},{5,4},{6,7},{7,6},{8,9},{9,8},{10,11... | collective-permute-start | bytes 1572872 | tf_op jit(solution)/shard_map/ppermute | solution.py:369
  136.8 30.4 %copy-start.9 = (bf16[128,2048]{1,0:T(8,128)(2,1)}, bf16[128,2048]{1,0:T(8,128)(2,1)S(1)}, u32[]{:S(2)}) copy-start(bf16[128,2048]{1,0:T(8,128)(2,1)S(1)} %collective-permute-done.3.x_ref) | copy-start | bytes 1572868
  136.8 18.3 %collective-permute-start.4 = (bf16[192,2048]{1,0:T(8,128)(2,1)S(1)}, bf16[192,2048]{1,0:T(8,128)(2,1)S(1)}, u32[]{:S(2)}, u32[]{:S(2)}) collective-permute-start(bf16[192,2048]{1,0:T(8,128)(2,1)S(1)} %get-tuple-element.28), channel_id=1, source_target_pairs={{0,1},{1,0},{2,3},{3,2},{4,5},{5,4},{6,7},{7,6},{8,9},{9,8},{10,11... | collective-permute-start | bytes 2359304 | tf_op jit(solution)/shard_map/ppermute | solution.py:369
  155.1 23.2 %copy-start.5 = (bf16[192,2048]{1,0:T(8,128)(2,1)}, bf16[192,2048]{1,0:T(8,128)(2,1)S(1)}, u32[]{:S(2)}) copy-start(bf16[192,2048]{1,0:T(8,128)(2,1)S(1)} %collective-permute-done.4.x_ref) | copy-start | bytes 2359300
  155.1 35.4 %collective-permute-start.5 = (bf16[192,2048]{1,0:T(8,128)(2,1)S(1)}, bf16[192,2048]{1,0:T(8,128)(2,1)S(1)}, u32[]{:S(2)}, u32[]{:S(2)}) collective-permute-start(bf16[192,2048]{1,0:T(8,128)(2,1)S(1)} %get-tuple-element.29), channel_id=1, source_target_pairs={{0,1},{1,0},{2,3},{3,2},{4,5},{5,4},{6,7},{7,6},{8,9},{9,8},{10,11... | collective-permute-start | bytes 2359304 | tf_op jit(solution)/shard_map/ppermute | solution.py:369
  190.6 13.0 %copy-start.10 = (bf16[128,2048]{1,0:T(8,128)(2,1)S(1)}, bf16[128,2048]{1,0:T(8,128)(2,1)}, u32[]{:S(2)}) copy-start(bf16[128,2048]{1,0:T(8,128)(2,1)} %shard_map.147) | copy-start | bytes 1572868
  190.6 14.4 %copy-start.4 = (bf16[192,2048]{1,0:T(8,128)(2,1)S(1)}, bf16[192,2048]{1,0:T(8,128)(2,1)}, u32[]{:S(2)}) copy-start(bf16[192,2048]{1,0:T(8,128)(2,1)} %shard_map.148) | copy-start | bytes 2359300
  190.6 0.9 copy-start.6
  203.5 21.3 %collective-permute-start.8 = (bf16[128,2048]{1,0:T(8,128)(2,1)S(1)}, bf16[128,2048]{1,0:T(8,128)(2,1)S(1)}, u32[]{:S(2)}, u32[]{:S(2)}) collective-permute-start(bf16[128,2048]{1,0:T(8,128)(2,1)S(1)} %copy-done.10), channel_id=1, source_target_pairs={{0,1},{1,0},{2,3},{3,2},{4,5},{5,4},{6,7},{7,6},{8,9},{9,8},{10,11... | collective-permute-start | bytes 1572872 | tf_op jit(solution)/shard_map/ppermute | solution.py:369
  205.0 30.2 %collective-permute-start.7 = (bf16[192,2048]{1,0:T(8,128)(2,1)S(1)}, bf16[192,2048]{1,0:T(8,128)(2,1)S(1)}, u32[]{:S(2)}, u32[]{:S(2)}) collective-permute-start(bf16[192,2048]{1,0:T(8,128)(2,1)S(1)} %copy-done.4), channel_id=1, source_target_pairs={{0,1},{1,0},{2,3},{3,2},{4,5},{5,4},{6,7},{7,6},{8,9},{9,8},{10,11... | collective-permute-start | bytes 2359304 | tf_op jit(solution)/shard_map/ppermute | solution.py:369
  205.6 45.8 %collective-permute-start.6 = (bf16[192,2048]{1,0:T(8,128)(2,1)}, bf16[192,2048]{1,0:T(8,128)(2,1)S(1)}, u32[]{:S(2)}, u32[]{:S(2)}) collective-permute-start(bf16[192,2048]{1,0:T(8,128)(2,1)} %shard_map.149), channel_id=1, source_target_pairs={{0,1},{1,0},{2,3},{3,2},{4,5},{5,4},{6,7},{7,6},{8,9},{9,8},{10,11... | collective-permute-start | bytes 2359304 | tf_op jit(solution)/shard_map/ppermute | solution.py:369
  224.8 0.8 copy-start.11
  235.2 0.9 copy-start.8
  251.3 0.9 copy-start.7
Sparse Core Ops, SparseCore 0:
  68.0 99.0 all-gather.1
